TPU v7x, 128 devices: a whole 4x4x4 slice. The times are simulated.
128 devices in a mesh: sp: 16 (over z, y), dp: 8 (over x, core).
Axes of the slice: x: 4, y: 4, z: 4, core: 2. Of those that a mesh axis runs over, the one named last changes fastest.
Arguments:
- u_pre: bfloat16 [8, 16384, 2048], P('dp', 'sp'), may hold values from -6 to 6
- v_pre: bfloat16 [8, 16384, 2048], P('dp', 'sp'), may hold values from -6 to 6
- d_out: bfloat16 [8, 16384, 2048], P('dp', 'sp'), may hold values from -6 to 6
- w_mix: bfloat16 [16, 128, 128], replicated, may hold values from -0.5 to 0.5
- mix_bias: float32 [16, 128], replicated, may hold values from 0.1 to 1.9
- norm_gain: float32 [16, 128], replicated, may hold values from 0.1 to 1.9
- norm_shift: float32 [16, 128], replicated, may hold values from -3 to 3
- w_out: bfloat16 [2048, 2048], P('dp'), may hold values from -0.125 to 0.125
Outputs:
- grad_u: bfloat16 [8, 16384, 2048], P('dp', 'sp')
- grad_v: bfloat16 [8, 16384, 2048], P('dp', 'sp')
- grad_w_out: float32 [2048, 2048], P('dp')
- grad_w_mix: float32 [16, 128, 128], replicated
- grad_mix_bias: float32 [16, 128], replicated
- grad_gain: float32 [16, 128], replicated
- grad_shift: float32 [16, 128], replicated
All inputs are finite; a program needn't handle non-finite values.
Results may differ from a plain program's by a relative error of at most 0.012.
Values may be sent and summed in bfloat16 or wider, within the bound.
A program may use at most 192 MiB of HBM per device.

v0:
```python
import jax
import jax.numpy as jnp
from jax import lax
from jax.sharding import PartitionSpec as P

EPS = 1e-05


def together(arrays, axis):
    ends = [0]
    for a in arrays:
        ends.append(ends[-1] + a.size)
    total = lax.psum(jnp.concatenate([a.ravel() for a in arrays]), axis)
    return tuple((total[b:e].reshape(a.shape) for a, b, e in zip(arrays, ends, ends[1:])))


def mechanism(grad_s, u_pre, v_pre, w_mix, mix_bias, gain, shift):
    items, length, width = grad_s.shape
    groups, span = (w_mix.shape[0], w_mix.shape[1])
    chans = width // groups
    shape = (items, length // span, span, groups, chans)
    u_val = u_pre.astype(jnp.float32).reshape(shape)
    v_val = v_pre.astype(jnp.float32).reshape(shape)
    cotan = grad_s.astype(jnp.float32).reshape(shape)
    upper, u_back = jax.vjp(jax.nn.gelu, u_val)
    gated, v_back = jax.vjp(jax.nn.gelu, v_val)
    centre = gated - jnp.mean(gated, axis=-1, keepdims=True)
    inverse = lax.rsqrt(jnp.mean(centre * centre, axis=-1, keepdims=True) + EPS)
    scaled = centre * inverse
    normed = (scaled * gain + shift).astype(jnp.bfloat16)
    lower = jnp.tril(jnp.ones((span, span), dtype=bool))
    w_low = jnp.where(lower[None], w_mix, jnp.zeros_like(w_mix))
    mixed = jnp.einsum("gts,insgc->intgc", w_low, normed, preferred_element_type=jnp.float32)
    mixed = mixed + jnp.transpose(mix_bias)[:, :, None]
    gated_out = (upper * mixed).astype(jnp.bfloat16)
    d_mixed = cotan * upper
    d_mixed_b = d_mixed.astype(jnp.bfloat16)
    grad_u = u_back(cotan * mixed)[0].astype(jnp.bfloat16).reshape(items, length, width)
    grad_bias = jnp.transpose(jnp.sum(d_mixed, axis=(0, 1, 4)))
    grad_w = jnp.einsum("intgc,insgc->gts", d_mixed_b, normed, preferred_element_type=jnp.float32)
    grad_w = jnp.where(lower[None], grad_w, jnp.zeros_like(grad_w))
    d_normed = jnp.einsum("gts,intgc->insgc", w_low, d_mixed_b, preferred_element_type=jnp.float32)
    grad_gain = jnp.sum(d_normed * scaled, axis=(0, 1, 2))
    grad_shift = jnp.sum(d_normed, axis=(0, 1, 2))
    d_scaled = d_normed * gain
    d_gated = inverse * (
        d_scaled
        - jnp.mean(d_scaled, axis=-1, keepdims=True)
        - scaled * jnp.mean(d_scaled * scaled, axis=-1, keepdims=True)
    )
    grad_v = v_back(d_gated)[0].astype(jnp.bfloat16).reshape(items, length, width)
    return (
        grad_u,
        grad_v,
        gated_out.reshape(items, length, width),
        grad_w,
        grad_bias,
        grad_gain,
        grad_shift,
    )


def on_device(u_pre, v_pre, d_out, w_mix, mix_bias, norm_gain, norm_shift, w_out):
    grad_s = lax.dot_general(
        d_out,
        lax.all_gather(w_out, "dp", axis=0, tiled=True),
        (((2,), (1,)), ((), ())),
        preferred_element_type=jnp.float32,
    ).astype(jnp.bfloat16)
    grad_u, grad_v, gated_out, grad_w, grad_bias, grad_gain, grad_shift = mechanism(
        grad_s, u_pre, v_pre, w_mix, mix_bias, norm_gain, norm_shift
    )
    grad_w, grad_bias, grad_gain, grad_shift = together(
        (grad_w, grad_bias, grad_gain, grad_shift), ("sp", "dp")
    )
    width = gated_out.shape[2]
    flat_d = d_out.reshape(-1, d_out.shape[2])
    flat_s = gated_out.reshape(-1, width)
    partial_rows = lax.psum_scatter(
        lax.dot_general(
            flat_s, flat_d, (((0,), (0,)), ((), ())), preferred_element_type=jnp.float32
        ),
        "dp",
        scatter_dimension=0,
        tiled=True,
    )
    grad_w_out = lax.psum(partial_rows, "sp")
    return (grad_u, grad_v, grad_w_out, grad_w, grad_bias, grad_gain, grad_shift)


def solution(mesh):
    return jax.shard_map(
        on_device,
        mesh=mesh,
        in_specs=(
            P("dp", "sp", None),
            P("dp", "sp", None),
            P("dp", "sp", None),
            P(),
            P(),
            P(),
            P(),
            P("dp", None),
        ),
        out_specs=(P("dp", "sp", None), P("dp", "sp", None), P("dp", None), P(), P(), P(), P()),
        check_vma=False,
    )
```

profile of v0, /device:TPU:0, one launch (start us, length us, event | category | flops | bytes accessed | tf_op | source)
XLA Modules:
  0.0 473.9 jit_solution(16673040196392679940)
XLA Ops:
  7.2 0.7 all-gather.2.cloned.1.call-update
  7.9 3.2 convert_bitcast_fusion
  11.2 5.2 %copy.67 = f32[128,8,16,128]{3,2,1,0:T(8,128)} copy(f32[128,8,16,128]{3,1,2,0:T(8,128)S(1)} %convert_bitcast_fusion) | data formatting | bytes 16777216
  16.4 9.5 %copy.45 = f32[1,8,128,16,128]{2,4,1,3,0:T(8,128)} copy(f32[1,8,128,16,128]{4,3,0,2,1:T(8,128)} %bitcast.100) | data formatting | bytes 16777216 | tf_op jit(solution)/shard_map/reshape | solution.py:22
  25.9 3.2 convert_bitcast_fusion.1
  29.1 5.2 %copy.65 = f32[128,8,16,128]{3,2,1,0:T(8,128)} copy(f32[128,8,16,128]{3,1,2,0:T(8,128)S(1)} %convert_bitcast_fusion.1) | data formatting | bytes 16777216
  34.3 8.7 %copy.39 = f32[1,8,128,16,128]{2,4,1,3,0:T(8,128)} copy(f32[1,8,128,16,128]{4,3,0,2,1:T(8,128)} %bitcast.104) | data formatting | bytes 16777216 | tf_op jit(solution)/shard_map/reshape | solution.py:23
  43.1 5.9 %fusion.54 = f32[8,128,16]{1,0,2:T(8,128)S(1)} fusion(f32[1,8,128,16,128]{2,4,1,3,0:T(8,128)} %copy.39), kind=kLoop, calls=%fused_computation.83 | loop fusion | flops 18857984 | bytes 8454144 | tf_op jit(solution)/shard_map/reduce_sum | solution.py:27
  49.2 3.7 multiply_reduce_fusion.2
  53.0 6.5 %fusion.35 = bf16[8,128,16,128]{3,1,0,2:T(8,128)(2,1)} fusion(f32[8,128,16,128]{3,2,1,0:T(8,128)S(1)} %bitcast.105, f32[16,128]{1,0:T(8,128)S(1)} %copy-done.4, f32[16,128]{1,0:T(8,128)S(1)} %copy-done.3, f32[8,128,16]{1,0,2:T(8,128)S(1)} %add_rsqrt_fusion, f32[8,128,16]{1,0,2:T(8,128)S(1)} %broadcast_multiply_fusion.2), kind=kLoop, calls=%fused_computation.52 | loop fusion | flops 27262976 | bytes 12730368 | tf_op jit(solution)/shard_map/convert_element_type | solution.py:30
  59.5 2.4 all-gather.2.cloned.1.call-done
  61.8 12.7 %convert_bitcast_fusion.2 = f32[128,8,16,128]{3,1,2,0:T(8,128)S(1)} fusion(bf16[2048,2048]{1,0:T(8,128)(2,1)} %all-gather.2.cloned.1.call-done, bf16[1,1024,2048]{2,1,0:T(8,128)(2,1)} %param.10), kind=kOutput, calls=%fused_computation.51 | convolution fusion | flops 8594128896 | bytes 20971520 | tf_op jit(solution)/shard_map/dot_general | solution.py:64
  74.6 5.2 %copy.64 = f32[128,8,16,128]{3,2,1,0:T(8,128)} copy(f32[128,8,16,128]{3,1,2,0:T(8,128)S(1)} %convert_bitcast_fusion.2) | data formatting | bytes 16777216
  79.8 8.8 %copy.41 = f32[1,8,128,16,128]{2,4,1,3,0:T(8,128)} copy(f32[1,8,128,16,128]{4,3,2,1,0:T(8,128)} %bitcast.102) | data formatting | bytes 16777216 | tf_op jit(solution)/shard_map/reshape | solution.py:24
  88.5 14.8 %multiply_convert_fusion = (bf16[1,8,128,16,128]{2,4,1,3,0:T(8,128)(2,1)}, bf16[1,8,128,16,128]{2,4,1,3,0:T(8,128)(2,1)}, f32[128,16]{0,1:T(8,128)S(1)}) fusion(f32[128,16]{0,1:T(8,128)S(1)} %bitcast.112, f32[1,8,128,16,128]{2,4,1,3,0:T(8,128)} %copy.45, f32[1,8,128,16,128]{2,4,1,3,0:T(8,128)} %copy.41, bf16[8,128,16,128]{3,1,0,2:T(8,128)(2,1)} %fusion.35, ...), kind=kOutput, calls=%fused_computation.46 | convolution fusion | flops 593754112 | bytes 29917184 | tf_op jit(solution)/shard_map/gts,insgc->intgc/dot_general | solution.py:33
  103.3 6.8 %copy.58 = bf16[1,8,128,16,128]{4,3,2,1,0:T(8,128)(2,1)} copy(bf16[1,8,128,16,128]{2,4,1,3,0:T(8,128)(2,1)} %get-tuple-element.11) | data formatting | bytes 8388608 | tf_op jit(solution)/shard_map/convert_element_type | solution.py:35
  110.1 15.4 %fusion.37 = f32[2048,2048]{1,0:T(8,128)} fusion(bf16[128,8,16,128]{3,2,1,0:T(8,128)(2,1)} %bitcast.107, bf16[1,1024,2048]{2,1,0:T(8,128)(2,1)} %param.10), kind=kOutput, calls=%fused_computation.57 | convolution fusion | flops 8589934592 | bytes 25165824 | tf_op jit(solution)/shard_map/dot_general | solution.py:80
  125.6 10.2 %fusion.33 = bf16[8,128,16,128]{3,1,0,2:T(8,128)(2,1)S(1)} fusion(f32[8,128,16,128]{3,2,1,0:T(8,128)} %bitcast.103, f32[8,128,16,128]{3,2,1,0:T(8,128)} %bitcast.101), kind=kLoop, calls=%fused_computation.39 | loop fusion | flops 20971520 | bytes 20971520 | tf_op jit(solution)/shard_map/convert_element_type | solution.py:37
  135.8 1.3 fusion.45
  137.1 10.3 %fusion.34 = (f32[16,128]{1,0:T(8,128)S(1)}, f32[8,128,16]{1,0,2:T(8,128)S(1)}, f32[8,128,16]{1,0,2:T(8,128)S(1)}, f32[16,128]{1,0:T(8,128)S(1)}, f32[16,8,128,128]{3,2,1,0:T(8,128)}) fusion(f32[8,128,16]{1,0,2:T(8,128)S(1)} %add_rsqrt_fusion, f32[8,128,16]{1,0,2:T(8,128)S(1)} %broadcast_multiply_fusion.2, f32[1,8,128,16,128]{2,4,1,3,0:T(8,128)} %copy.39, ...), kind=kOutput, calls=%fused_computation.44 | convolution fusion | flops 572747776 | bytes 21798912 | tf_op jit(solution)/shard_map/gts,intgc->insgc/dot_general | solution.py:42
  147.4 1.0 pad_maximum_fusion
  148.6 7.0 %copy.47 = bf16[1,8,128,16,128]{4,3,2,1,0:T(8,128)(2,1)} copy(bf16[1,8,128,16,128]{2,4,1,3,0:T(8,128)(2,1)} %get-tuple-element.12) | data formatting | bytes 8388608 | tf_op jit(solution)/shard_map/convert_element_type | solution.py:38
  155.6 7.3 %reshape.497 = bf16[1,1024,2048]{2,1,0:T(8,128)(2,1)} reshape(bf16[1,8,128,16,128]{4,3,2,1,0:T(8,128)(2,1)} %copy.47) | data formatting | bytes 8388608 | tf_op jit(solution)/shard_map/reshape | solution.py:38
  162.9 54.8 %reduce-scatter.2.cloned.1.call-done = f32[256,2048]{1,0:T(8,128)} async-done(((f32[2048,2048]{1,0:T(8,128)}), f32[256,2048]{1,0:T(8,128)}) %reduce-scatter.2.cloned.1.call-update) | async-done | bytes 2097168 | tf_op jit(solution)/shard_map/reduce_scatter | solution.py:79
  217.7 12.0 %fusion.6 = bf16[1,8,128,16,128]{2,4,1,3,0:T(8,128)(2,1)} fusion(f32[1,8,128,16,128]{2,4,1,3,0:T(8,128)} %copy.39, f32[16,8,128,128]{3,2,1,0:T(8,128)} %get-tuple-element.17, f32[8,128,16]{1,0,2:T(8,128)S(1)} %get-tuple-element.18, f32[8,128,16]{1,0,2:T(8,128)S(1)} %get-tuple-element.19, f32[16,128]{1,0:T(8,128)S(1)} %copy-done.3, ...), kind=kLoop, calls=%fused_computation.12 | loop fusion | flops 58720256 | bytes 21241856 | tf_op jit(solution)/shard_map/convert_element_type | solution.py:51
  229.8 6.7 %copy.56 = bf16[1,8,128,16,128]{4,3,2,1,0:T(8,128)(2,1)} copy(bf16[1,8,128,16,128]{2,4,1,3,0:T(8,128)(2,1)} %fusion.6) | data formatting | bytes 8388608 | tf_op jit(solution)/shard_map/convert_element_type | solution.py:51
  236.5 7.3 %reshape.500 = bf16[1,1024,2048]{2,1,0:T(8,128)(2,1)} reshape(bf16[1,8,128,16,128]{4,3,2,1,0:T(8,128)(2,1)} %copy.56) | data formatting | bytes 8388608 | tf_op jit(solution)/shard_map/reshape | solution.py:51
  243.8 127.2 %all-reduce.5.cloned.1.call-done = f32[268288]{0:T(1024)} async-done(((f32[268288]{0:T(1024)}), f32[268288]{0:T(1024)}) %all-reduce.5.cloned.1.call-update) | async-done | bytes 1073168 | tf_op jit(solution)/shard_map/psum | solution.py:13
  371.0 2.3 slice.49
  373.2 1.3 slice_bitcast_fusion
  374.6 89.4 %all-reduce.3.cloned.1.call-done = f32[256,2048]{1,0:T(8,128)} async-done(((f32[256,2048]{1,0:T(8,128)}), f32[256,2048]{1,0:T(8,128)}) %all-reduce.3.cloned.1.call-update) | async-done | bytes 2097168 | tf_op jit(solution)/shard_map/psum | solution.py:87
  464.0 3.1 copy.82
  (25 shorter events, 0.5 us)
Async XLA Ops:
  7.2 54.7 %all-gather.2.cloned.1.call-start = ((), (), s32[]{:S(2)}) async-start(), calls=%async_computation.1 | async-start | bytes 9437184 | tf_op jit(solution)/shard_map/all_gather | solution.py:66
  7.9 209.8 %reduce-scatter.2.cloned.1.call-start = ((), (), s32[]{:S(2)}) async-start(), calls=%async_computation.2 | async-start | bytes 18874368 | tf_op jit(solution)/shard_map/reduce_scatter | solution.py:79
  43.0 6.2 %copy-start = (f32[1,8,128,16,128]{2,4,1,3,0:T(8,128)S(1)}, f32[1,8,128,16,128]{2,4,1,3,0:T(8,128)}, u32[]{:S(2)}) copy-start(f32[1,8,128,16,128]{2,4,1,3,0:T(8,128)} %copy.39) | copy-start | bytes 25165828
  43.0 9.9 %copy-start.1 = (f32[128,8,16,128]{3,2,1,0:T(8,128)S(1)}, f32[128,8,16,128]{3,2,1,0:T(8,128)}, u32[]{:S(2)}) copy-start(f32[128,8,16,128]{3,2,1,0:T(8,128)} %copy.65) | copy-start | bytes 25165828
  43.1 9.9 %copy-start.3 = (f32[16,128]{1,0:T(8,128)S(1)}, f32[16,128]{1,0:T(8,128)}, u32[]{:S(2)}) copy-start(f32[16,128]{1,0:T(8,128)} %param.13) | copy-start | bytes 24580
  43.1 9.9 %copy-start.4 = (f32[16,128]{1,0:T(8,128)S(1)}, f32[16,128]{1,0:T(8,128)}, u32[]{:S(2)}) copy-start(f32[16,128]{1,0:T(8,128)} %param.14) | copy-start | bytes 24580
  79.7 8.8 %copy-start.5 = (bf16[16,128,128]{2,1,0:T(8,128)(2,1)S(1)}, bf16[16,128,128]{2,1,0:T(8,128)(2,1)}, u32[]{:S(2)}) copy-start(bf16[16,128,128]{2,1,0:T(8,128)(2,1)} %param.11) | copy-start | bytes 1572868
  79.8 8.8 %copy-start.6 = (f32[16,128]{1,0:T(8,128)S(1)}, f32[16,128]{1,0:T(8,128)}, u32[]{:S(2)}) copy-start(f32[16,128]{1,0:T(8,128)} %param.12) | copy-start | bytes 24580
  125.6 245.4 %all-reduce.5.cloned.1.call-start = ((), (), s32[]{:S(2)}) async-start(), calls=%async_computation.4 | async-start | bytes 2146304 | tf_op jit(solution)/shard_map/psum | solution.py:13
  125.6 10.2 %copy-start.2 = (bf16[8,128,16,128]{3,1,0,2:T(8,128)(2,1)S(1)}, bf16[8,128,16,128]{3,1,0,2:T(8,128)(2,1)}, u32[]{:S(2)}) copy-start(bf16[8,128,16,128]{3,1,0,2:T(8,128)(2,1)} %fusion.35) | copy-start | bytes 12582916
  148.5 315.5 %all-reduce.3.cloned.1.call-start = ((), (), s32[]{:S(2)}) async-start(), calls=%async_computation.3 | async-start | bytes 4194304 | tf_op jit(solution)/shard_map/psum | solution.py:87
Sparse Core Ops, SparseCore 0:
  9.7 52.0 all-gather.1
  125.7 91.9 reduce-scatter.1
  223.1 147.8 all-reduce.4
  374.2 89.7 all-reduce.2
where the time goes:
time: 478 us; the launch traced here: 474 us
  waiting for transfers between devices  274 us (57%)
  local copies, waits for them, and re-layouts  84.7 us (18%)
  matrix products  54.5 us (11%)
  other arithmetic  45.8 us (10%)
  between operations  14.2 us (3%)
    psum x1, waiting for transfers between devices, together(): total = lax.psum(jnp.concatenate([a.ravel() for a in arrays]), axis)  127 us
    psum x1, waiting for transfers between devices, on_device(): grad_w_out = lax.psum(partial_rows, 'sp')  89.4 us
    reduce_scatter x1, waiting for transfers between devices, on_device(): lax.psum_scatter(lax.dot_general(flat_s, flat_d, (((0,), (0,)), ((), ()))...  54.8 us
    unnamed x18, local copies, waits for them, and re-layouts  19 us
    dot_general x1, matrix products, on_device(): lax.dot_general(flat_s, flat_d, (((0,), (0,)), ((), ())), preferred_eleme...  15.4 us
    dot_general x1, matrix products, mechanism(): jnp.einsum('gts,insgc->intgc', w_low, normed, preferred_element_type=jnp....  14.8 us
    dot_general x1, matrix products, on_device(): lax.dot_general(d_out, lax.all_gather(w_out, 'dp', axis=0, tiled=True), (...  12.7 us
    convert_element_type x1, other arithmetic, mechanism(): v_back(d_gated)[0].astype(jnp.bfloat16).reshape(items, length, width)  12 us
  transfers between devices with their start and end apart: 4, of which 4 were waited for; matrix products, arithmetic and copies ran while one was open for 25% of the time, Pallas kernels for 0%

commit v1 on v0

v1 whole, which is shorter than its diff:
```python
import functools

import jax
import jax.numpy as jnp
from jax import lax
from jax.experimental import pallas as pl
from jax.experimental.pallas import tpu as pltpu
from jax.sharding import PartitionSpec as P

EPS = 1e-05
C0 = 0.7978845608028654
C1 = 0.044715
F32 = jnp.float32
BF = jnp.bfloat16
MESH = pl.DeviceIdType.MESH
WID = 2048
EXT = WID + 128


def rdma(src, dst, ssem, rsem, dev):
    return pltpu.make_async_remote_copy(
        src_ref=src, dst_ref=dst, send_sem=ssem, recv_sem=rsem, device_id=dev, device_id_type=MESH
    )


def al(v, m):
    return pl.multiple_of(v, m)


def gelu_pair(a):
    a2 = a * a
    th = jnp.tanh(a * (C0 + (C0 * C1) * a2))
    s = 0.5 + 0.5 * th
    g = a * s
    slope = s + g * (1.0 - s) * (2.0 * C0 + (6.0 * C0 * C1) * a2)
    return g, slope


def lane_mean(a):
    return jnp.sum(a, axis=-1, keepdims=True) * (1.0 / 128.0)


def dot_nn(a, b):
    return lax.dot_general(a, b, (((1,), (0,)), ((), ())), preferred_element_type=F32)


def dot_nt(a, b):
    return lax.dot_general(a, b, (((1,), (1,)), ((), ())), preferred_element_type=F32)


def kernel(
    u_hbm, v_hbm, d_hbm, wm_ref, bias_ref, gain_ref, shift_ref, w_hbm,
    gu_hbm, gv_hbm, gw_hbm, gm_hbm, gb_ref, gg_ref, gsh_ref,
    d_v, wbuf, ub, vb, gub, gvb, gs, gt, pb, pr, tb, r1, q, r2, vx, rx, ob, of,
    cb, rc1, qc, rc2, qd, rc3, cg, cp, gm,
    st, st2, rs0, rs1, wl, wlt, bb, gwacc, bacc, gacc, sacc,
    ld_s, uv_s, out_s, wsend, wrecv, wrel_s, wrel_r,
    ps_s, ps_r, s1_s, s1_r, s2_s, s2_r, x_s, x_r, g1_s, g1_r, g2_s, g2_r,
    c_s, c_r, t_s, t_r, fin_s,
):
    sp = lax.axis_index("sp")
    dp = lax.axis_index("dp")
    z, y = sp // 4, sp % 4
    x, c = dp // 2, dp % 2
    o = 1 - c

    def dev(x_, y_, z_, c_):
        return (z_ * 4 + y_, x_ * 2 + c_)

    def px(d):
        return dev((x + d) % 4, y, z, c)

    def py(d):
        return dev(x, (y + d) % 4, z, c)

    def pz(d):
        return dev(x, y, (z + d) % 4, c)

    mate = dev(x, y, z, o)
    first = (py, pz)
    second = (pz, py)
    i1 = (y, z)
    i2 = (z, y)

    own = [
        pltpu.make_async_copy(w_hbm.at[pl.ds(g * 128, 128)], wbuf.at[g, c], ld_s.at[g]) for g in range(2)
    ]
    dcp = [
        pltpu.make_async_copy(
            d_hbm.at[0, pl.ds(i * 256, 256)], d_v.at[pl.ds(i * 256, 256)], ld_s.at[2 + i]
        )
        for i in range(4)
    ]
    for cpy in own:
        cpy.start()
    for cpy in dcp:
        cpy.start()

    def unit(u):
        par = u % 2
        quad = u // 2
        base = jnp.where(quad == 1, 3, jnp.where(quad == 2, 1, jnp.where(quad == 3, 2, 0)))
        xu = (x + base + par * quad * (3 - quad)) % 4
        return xu, par, quad

    def cols(u, cls):
        xu, par, _ = unit(u)
        return pl.ds(al((4 * xu + 2 * cls + par) * 128, 128), 128)

    def uv_copies(u):
        slot = u % 2
        res = []
        for k, (hbm, buf) in enumerate(((u_hbm, ub), (v_hbm, vb))):
            for cls in range(2):
                res.append(
                    pltpu.make_async_copy(
                        hbm.at[0, :, cols(u, cls)],
                        buf.at[slot, :, pl.ds(cls * 128, 128)],
                        uv_s.at[slot, k, cls],
                    )
                )
        return res

    def out_copies(u):
        slot = u % 2
        res = []
        for k, (hbm, buf) in enumerate(((gu_hbm, gub), (gv_hbm, gvb))):
            for cls in range(2):
                res.append(
                    pltpu.make_async_copy(
                        buf.at[slot, :, pl.ds(cls * 128, 128)],
                        hbm.at[0, :, cols(u, cls)],
                        out_s.at[slot, k, cls],
                    )
                )
        return res

    for cpy in uv_copies(0):
        cpy.start()

    barrier = pltpu.get_barrier_semaphore()
    for peer in [mate] + [f(d) for f in (px, py, pz) for d in (1, 2, 3)]:
        pl.semaphore_signal(barrier, inc=1, device_id=peer, device_id_type=MESH)
    pl.semaphore_wait(barrier, 10)

    def wx(k):
        src, dst, d = ((0, 2, 1), (1, 3, 3), (1, 5, 1), (0, 4, 3), (2, 6, 1), (3, 7, 3))[k]
        return rdma(wbuf.at[src, c], wbuf.at[dst, c], wsend.at[k], wrecv.at[k], px(d))

    arrival = {2: 0, 3: 1, 5: 2, 4: 3, 6: 4, 7: 5}

    def relay(s, k):
        return rdma(wbuf.at[s, k], wbuf.at[s, k], wrel_s.at[s], wrel_r.at[s], mate)

    for cpy in own:
        cpy.wait()
    relay(0, c).start()
    relay(1, c).start()
    for k in range(4):
        wx(k).start()

    tri = lax.broadcasted_iota(jnp.int32, (128, 128), 0) >= lax.broadcasted_iota(jnp.int32, (128, 128), 1)

    def prep(g, _):
        w = jnp.where(tri, wm_ref[g].astype(F32), 0.0)
        wl[g] = w.astype(BF)
        wlt[g] = w.T.astype(BF)
        row = bias_ref[pl.ds(g, 1), :]
        bb[g] = jnp.broadcast_to(row, (128, 128)).T
        return 0

    lax.fori_loop(0, 16, prep, 0)
    for cpy in dcp:
        cpy.wait()

    def ps(u):
        return rdma(pb.at[u % 2, o], pr.at[u], ps_s.at[u % 2], ps_r.at[u], mate)

    def s1(u, ab, d, j):
        return rdma(
            tb.at[u % 2, pl.ds(al(32 * j, 32), 32), pl.ds(1024 * ab, 1024)],
            r1.at[u, ab, d - 1],
            s1_s.at[u % 2, ab, d - 1],
            s1_r.at[u, ab, d - 1],
            first[ab](d),
        )

    def s2(u, ab, d, j):
        return rdma(
            q.at[u % 2, ab, :, pl.ds(al(256 * j, 256), 256)],
            r2.at[u, ab, d - 1],
            s2_s.at[u % 2, ab, d - 1],
            s2_r.at[u, ab, d - 1],
            second[ab](d),
        )

    def xs(u):
        xu, par, quad = unit(u)
        return rdma(vx.at[u], rx.at[par, quad], x_s.at[u], x_r.at[par, quad], dev(xu, y, z, c))

    PAIRS = [(ab, d) for ab in range(2) for d in (1, 2, 3)]

    def do_ts(u):
        ps(u).wait()
        slot = u % 2
        xu, par, _ = unit(u)

        def body(i, _):
            r = pl.ds(al(i * 16, 16), 16)
            tb[slot, r, :] = (
                pb[slot, c, r, pl.ds(0, WID)].astype(F32) + pr[u, r, pl.ds(0, WID)].astype(F32)
            ).astype(BF)
            return 0

        lax.fori_loop(0, 8, body, 0)
        cb[xu * 2 + par] = (
            pb[slot, c, :, pl.ds(WID, 128)].astype(F32) + pr[u, :, pl.ds(WID, 128)].astype(F32)
        ).astype(BF)
        for ab, d in PAIRS:
            s1(u, ab, d, (i1[ab] + d) % 4).start()

    def do_s2(u):
        slot = u % 2
        for ab, d in PAIRS:
            s1(u, ab, d, (i1[ab] + d) % 4).wait()
        for ab in range(2):
            for h in range(2):
                r = pl.ds(16 * h, 16)
                acc = tb[slot, pl.ds(al(32 * i1[ab] + 16 * h, 16), 16), pl.ds(1024 * ab, 1024)].astype(F32)
                for k in range(3):
                    acc = acc + r1[u, ab, k, r, :].astype(F32)
                q[slot, ab, r, :] = acc.astype(BF)
        for ab, d in PAIRS:
            s2(u, ab, d, (i2[ab] + d) % 4).start()

    def do_x(u):
        slot = u % 2
        _, par, _ = unit(u)
        for ab, d in PAIRS:
            s2(u, ab, d, (i2[ab] + d) % 4).wait()
        for ab in range(2):
            acc = q[slot, ab, :, pl.ds(al(256 * i2[ab], 256), 256)].astype(F32)
            for k in range(3):
                acc = acc + r2[u, ab, k].astype(F32)
            vx[u, ab] = acc.astype(BF)

        @pl.when(u >= 2)
        def _():
            xs(u).start()

    def ob_small(g, ab, j):
        return ob.at[
            pl.ds(al(g * 128 + 32 * i1[ab], 32), 32), pl.ds(al(1024 * ab + 256 * j, 256), 256)
        ]

    def ob_big(g, ab, j):
        return ob.at[pl.ds(al(g * 128 + 32 * j, 32), 32), pl.ds(1024 * ab, 1024)]

    def g1(g, ab, d, j):
        return rdma(
            ob_small(g, ab, j), ob_small(g, ab, j), g1_s.at[g, ab, d - 1], g1_r.at[g, ab, d - 1], second[ab](d)
        )

    def g2(g, ab, d, j):
        return rdma(
            ob_big(g, ab, j), ob_big(g, ab, j), g2_s.at[g, ab, d - 1], g2_r.at[g, ab, d - 1], first[ab](d)
        )

    def do_f(g):
        for k in (1, 2, 3):
            rdma(vx.at[g], rx.at[g, k], x_s.at[g], x_r.at[g, k], mate).wait_recv()
        for ab in range(2):
            acc = vx[g, ab].astype(F32)
            for k in (1, 2, 3):
                acc = acc + rx[g, k, ab].astype(F32)
            ob_small(g, ab, i2[ab])[...] = acc.astype(BF)
        for ab, d in PAIRS:
            g1(g, ab, d, i2[ab]).start()

    def do_g2(g):
        for ab, d in PAIRS:
            g1(g, ab, d, (i2[ab] + 4 - d) % 4).wait_recv()
        for ab, d in PAIRS:
            g2(g, ab, d, i1[ab]).start()

    def out_w(g):
        return pltpu.make_async_copy(
            of.at[pl.ds(g * 128, 128)], gw_hbm.at[pl.ds(g * 128, 128)], fin_s.at[g]
        )

    def do_out(g):
        for ab, d in PAIRS:
            g2(g, ab, d, (i1[ab] + 4 - d) % 4).wait_recv()

        def body(i, _):
            r = pl.ds(al(g * 128 + i * 16, 16), 16)
            of[r, :] = ob[r, :].astype(F32)
            return 0

        lax.fori_loop(0, 8, body, 0)
        out_w(g).start()

    def arrive(s):
        wx(arrival[s]).wait_recv()
        relay(s, c).start()

    def unit_body(u, _):
        slot = u % 2
        xu, par, _q = unit(u)
        relay(u, o).wait_recv()

        @pl.when(u < 7)
        def _():
            for cpy in uv_copies(u + 1):
                cpy.start()

        def gs_body(i, _):
            r = pl.ds(al(i * 512, 512), 512)
            gs[r, :] = dot_nt(d_v[r, :], wbuf[u].reshape(256, WID)).astype(BF)
            return 0

        lax.fori_loop(0, 2, gs_body, 0)

        @pl.when(u >= 2)
        def _():
            do_x(u - 2)

        @pl.when(u >= 1)
        def _():
            do_ts(u - 1)

        for cpy in uv_copies(u):
            cpy.wait()

        @pl.when(u >= 2)
        def _():
            for cpy in out_copies(u - 2):
                cpy.wait()

        gwacc[...] = jnp.zeros_like(gwacc)
        bacc[...] = jnp.zeros_like(bacc)
        gacc[...] = jnp.zeros_like(gacc)
        sacc[...] = jnp.zeros_like(sacc)

        def block(n, _):
            r = pl.ds(al(n * 128, 128), 128)
            for cls in range(2):
                grp = 4 * xu + 2 * cls + par
                ln = pl.ds(cls * 128, 128)
                gain = gain_ref[pl.ds(grp, 1), :]
                shift = shift_ref[pl.ds(grp, 1), :]
                gated, v_slope = gelu_pair(vb[slot, r, ln].astype(F32))
                cen = gated - lane_mean(gated)
                inv = lax.rsqrt(lane_mean(cen * cen) + EPS)
                scaled = cen * inv
                nb = (scaled * gain + shift).astype(BF)
                upper, u_slope = gelu_pair(ub[slot, r, ln].astype(F32))
                cot = gs[r, ln].astype(F32)
                dm = cot * upper
                dmb = dm.astype(BF)
                bacc[cls] += dm
                mixed = dot_nn(wl[grp], nb) + bb[grp]
                dn = dot_nn(wlt[grp], dmb)
                gwacc[cls] += dot_nt(dmb, nb)
                gt[pl.ds(cls * 128, 128), r] = (upper * mixed).T.astype(BF)
                gub[slot, r, ln] = (cot * mixed * u_slope).astype(BF)
                prod = dn * scaled
                gacc[cls] += jnp.sum(prod.reshape(16, 8, 128), axis=0)
                sacc[cls] += jnp.sum(dn.reshape(16, 8, 128), axis=0)
                e = dn * gain
                m1 = lane_mean(e)
                m2 = lane_mean(prod * gain)
                gvb[slot, r, ln] = ((e - m1 - scaled * m2) * (v_slope * inv)).astype(BF)
            return 0

        lax.fori_loop(0, 8, block, 0)
        for cpy in out_copies(u):
            cpy.start()

        @pl.when(u >= 1)
        def _():
            do_s2(u - 1)

        def p_body(j, _):
            cl = pl.ds(al(j * 256, 256), 256)
            pb[slot, :, :, cl] = dot_nn(gt[...], d_v[:, cl]).astype(BF).reshape(2, 128, 256)
            return 0

        lax.fori_loop(0, 8, p_body, 0)
        for cls in range(2):
            grp = 4 * xu + 2 * cls + par
            pb[slot, cls, :, pl.ds(WID, 128)] = jnp.where(tri, gwacc[cls], 0.0).astype(BF)
            st[0, pl.ds(grp, 1), :] = jnp.sum(bacc[cls].T, axis=0, keepdims=True)
            st[1, pl.ds(grp, 1), :] = jnp.sum(gacc[cls], axis=0, keepdims=True)
            st[2, pl.ds(grp, 1), :] = jnp.sum(sacc[cls], axis=0, keepdims=True)
        ps(u).start()

        @pl.when(u == 1)
        def _():
            arrive(2)
            wx(4).start()
            arrive(3)
            wx(5).start()

        @pl.when(u == 3)
        def _():
            arrive(4)
            arrive(5)

        @pl.when(u == 5)
        def _():
            arrive(6)
            arrive(7)

        return 0

    lax.fori_loop(0, 8, unit_body, 0)

    def stat_sum(src, parts, dst):
        acc = src[...]
        for part in parts:
            acc = acc + part[...]
        dst[...] = acc

    t0 = rdma(st, rs0, t_s.at[0, 0], t_r.at[0, 0], mate)
    t0.start()

    def tstage(k, d, src, f):
        return rdma(src, rs1.at[k, d - 1], t_s.at[k + 1, d - 1], t_r.at[k + 1, d - 1], f(d))

    def cy(d, j):
        return rdma(
            cb.at[:, pl.ds(al(32 * j, 32), 32)], rc1.at[d - 1], c_s.at[0, d - 1], c_r.at[0, d - 1], py(d)
        )

    def cz(d, j):
        return rdma(qc.at[pl.ds(2 * j, 2)], rc2.at[d - 1], c_s.at[1, d - 1], c_r.at[1, d - 1], pz(d))

    def cx(d):
        return rdma(qd, rc3.at[d - 1], c_s.at[2, d - 1], c_r.at[2, d - 1], px(d))

    def cgz(d, j):
        ref = cg.at[pl.ds(2 * j, 2), pl.ds(al(32 * y, 32), 32)]
        return rdma(ref, ref, c_s.at[3, d - 1], c_r.at[3, d - 1], pz(d))

    def cgy(d, j):
        ref = cg.at[:, pl.ds(al(32 * j, 32), 32)]
        return rdma(ref, ref, c_s.at[4, d - 1], c_r.at[4, d - 1], py(d))

    DS = (1, 2, 3)
    do_x(6)
    do_ts(7)
    for d in DS:
        cy(d, (y + d) % 4).start()
    t0.wait()
    stat_sum(st, [rs0], st2.at[0])
    for d in DS:
        tstage(0, d, st2.at[0], py).start()
    do_f(0)
    do_s2(7)
    for d in DS:
        cy(d, (y + d) % 4).wait()
    acc = cb[:, pl.ds(al(32 * y, 32), 32), :].astype(F32)
    for k in range(3):
        acc = acc + rc1[k].astype(F32)
    qc[...] = acc.astype(BF)
    for d in DS:
        cz(d, (z + d) % 4).start()
    for d in DS:
        tstage(0, d, st2.at[0], py).wait()
    stat_sum(st2.at[0], [rs1.at[0, k] for k in range(3)], st2.at[1])
    for d in DS:
        tstage(1, d, st2.at[1], pz).start()
    do_g2(0)
    do_x(7)
    for d in DS:
        cz(d, (z + d) % 4).wait()
    acc = qc[pl.ds(2 * z, 2)].astype(F32)
    for k in range(3):
        acc = acc + rc2[k].astype(F32)
    qd[...] = acc.astype(BF)
    for d in DS:
        cx(d).start()
    for d in DS:
        tstage(1, d, st2.at[1], pz).wait()
    stat_sum(st2.at[1], [rs1.at[1, k] for k in range(3)], st2.at[2])
    for d in DS:
        tstage(2, d, st2.at[2], px).start()
    do_f(1)
    for d in DS:
        cx(d).wait()
    acc = qd[...].astype(F32)
    for k in range(3):
        acc = acc + rc3[k].astype(F32)
    cg[pl.ds(2 * z, 2), pl.ds(al(32 * y, 32), 32), :] = acc.astype(BF)
    for d in DS:
        cgz(d, z).start()
    do_out(0)
    for d in DS:
        tstage(2, d, st2.at[2], px).wait()
    tot = st2[2]
    for k in range(3):
        tot = tot + rs1[2, k]
    gb_ref[...] = tot[0]
    gg_ref[...] = tot[1]
    gsh_ref[...] = tot[2]
    do_g2(1)
    for d in DS:
        cgz(d, (z + 4 - d) % 4).wait_recv()
    for d in DS:
        cgy(d, y).start()
    for d in DS:
        cgy(d, (y + 4 - d) % 4).wait_recv()
    swap = rdma(cg, cp, c_s.at[5, 0], c_r.at[5, 0], mate)
    swap.start()

    def gm_body(src, cls):
        def body(i, _):
            gm[(i // 2) * 4 + 2 * cls + i % 2] = src[i].astype(F32)
            return 0

        lax.fori_loop(0, 8, body, 0)

    gm_body(cg, c)
    do_out(1)
    swap.wait()
    gm_body(cp, o)
    gmc = pltpu.make_async_copy(gm, gm_hbm, fin_s.at[2])
    gmc.start()

    for k in range(6):
        wx(k).wait_send()
    for s in range(8):
        relay(s, c).wait_send()
    for u in range(2, 8):
        xs(u).wait_send()
    for g in range(2):
        for ab, d in PAIRS:
            g1(g, ab, d, i2[ab]).wait_send()
            g2(g, ab, d, i1[ab]).wait_send()
    for d in DS:
        cgz(d, z).wait_send()
        cgy(d, y).wait_send()
    for u in (6, 7):
        for cpy in out_copies(u):
            cpy.wait()
    out_w(0).wait()
    out_w(1).wait()
    gmc.wait()


def on_device(u_pre, v_pre, d_out, w_mix, mix_bias, norm_gain, norm_shift, w_out):
    hbm = pl.BlockSpec(memory_space=pl.ANY)
    vm = pl.BlockSpec(memory_space=pltpu.VMEM)
    V = pltpu.VMEM
    DMA = pltpu.SemaphoreType.DMA
    scratch = [
        V((1024, WID), BF), V((8, 2, 128, WID), BF),
        V((2, 1024, 256), BF), V((2, 1024, 256), BF), V((2, 1024, 256), BF), V((2, 1024, 256), BF),
        V((1024, 256), BF), V((256, 1024), BF),
        V((2, 2, 128, EXT), BF), V((8, 128, EXT), BF), V((2, 128, WID), BF),
        V((8, 2, 3, 32, 1024), BF), V((2, 2, 32, 1024), BF), V((8, 2, 3, 32, 256), BF),
        V((8, 2, 32, 256), BF), V((2, 4, 2, 32, 256), BF), V((256, WID), BF), V((256, WID), F32),
        V((8, 128, 128), BF), V((3, 8, 32, 128), BF), V((8, 32, 128), BF), V((3, 2, 32, 128), BF),
        V((2, 32, 128), BF), V((3, 2, 32, 128), BF), V((8, 128, 128), BF), V((8, 128, 128), BF),
        V((16, 128, 128), F32),
        V((3, 16, 128), F32), V((3, 3, 16, 128), F32), V((3, 16, 128), F32), V((3, 3, 3, 16, 128), F32),
        V((16, 128, 128), BF), V((16, 128, 128), BF), V((16, 128, 128), F32),
        V((2, 128, 128), F32), V((2, 128, 128), F32), V((2, 8, 128), F32), V((2, 8, 128), F32),
        DMA((6,)), DMA((2, 2, 2)), DMA((2, 2, 2)), DMA((6,)), DMA((6,)), DMA((8,)), DMA((8,)),
        DMA((2,)), DMA((8,)), DMA((2, 2, 3)), DMA((8, 2, 3)), DMA((2, 2, 3)), DMA((8, 2, 3)),
        DMA((8,)), DMA((2, 4)), DMA((2, 2, 3)), DMA((2, 2, 3)), DMA((2, 2, 3)), DMA((2, 2, 3)),
        DMA((6, 3)), DMA((6, 3)), DMA((4, 3)), DMA((4, 3)), DMA((3,)),
    ]
    outs = pl.pallas_call(
        kernel,
        out_shape=(
            jax.ShapeDtypeStruct(u_pre.shape, BF),
            jax.ShapeDtypeStruct(v_pre.shape, BF),
            jax.ShapeDtypeStruct((256, WID), F32),
            jax.ShapeDtypeStruct((16, 128, 128), F32),
            jax.ShapeDtypeStruct((16, 128), F32),
            jax.ShapeDtypeStruct((16, 128), F32),
            jax.ShapeDtypeStruct((16, 128), F32),
        ),
        in_specs=[hbm, hbm, hbm, vm, vm, vm, vm, hbm],
        out_specs=(hbm, hbm, hbm, hbm, vm, vm, vm),
        scratch_shapes=scratch,
        compiler_params=pltpu.CompilerParams(
            collective_id=0, has_side_effects=True, vmem_limit_bytes=60 * 1024 * 1024
        ),
    )(u_pre, v_pre, d_out, w_mix, mix_bias, norm_gain, norm_shift, w_out)
    return outs


def solution(mesh):
    return jax.shard_map(
        on_device,
        mesh=mesh,
        in_specs=(
            P("dp", "sp", None), P("dp", "sp", None), P("dp", "sp", None),
            P(), P(), P(), P(), P("dp", None),
        ),
        out_specs=(P("dp", "sp", None), P("dp", "sp", None), P("dp", None), P(), P(), P(), P()),
        check_vma=False,
    )
```

time: 478 us -> 144 us (0.30)
  waiting for transfers between devices: 274 us -> 0 us
  Pallas kernels: 0 us -> 130 us
  local copies, waits for them, and re-layouts: 84.7 us -> 12.7 us
  matrix products: 54.5 us -> 0 us
  other arithmetic: 45.8 us -> 0 us
  between operations: 14.2 us -> 0.66 us
    psum x2 -> x0, waiting for transfers between devices: 217 us -> none  [the longest x1 127 us: together(): total = lax.psum(jnp.concatenate([a.ravel() for a in arrays]), axis)]
    pallas_call x0 -> x1, Pallas kernels: none -> 130 us  [on_device(): pl.pallas_call(kernel, out_shape=(jax.ShapeDtypeStruct(u_pre.shape, BF),...]
    reduce_scatter x1 -> x0, waiting for transfers between devices: 54.8 us -> none  [on_device(): lax.psum_scatter(lax.dot_general(flat_s, flat_d, (((0,), (0,)), ((), ()))...]
    dot_general x5 -> x0, matrix products: 54.5 us -> none  [the longest x1 15.4 us: on_device(): lax.dot_general(flat_s, flat_d, (((0,), (0,)), ((), ())), preferred_eleme...]
    reshape x5 -> x0, local copies, waits for them, and re-layouts: 41.6 us -> none  [the longest x1 9.49 us: mechanism(): u_val = u_pre.astype(jnp.float32).reshape(shape)]
    convert_element_type x3 -> x0, other arithmetic: 28.7 us -> none  [the longest x1 12 us: mechanism(): v_back(d_gated)[0].astype(jnp.bfloat16).reshape(items, length, width)]
    convert_element_type x3 -> x0, local copies, waits for them, and re-layouts: 20.5 us -> none  [the longest x1 7 us: mechanism(): u_back(cotan * mixed)[0].astype(jnp.bfloat16).reshape(items, length, width)]
    reduce_sum x2 -> x0, other arithmetic: 9.6 us -> none  [the longest x1 5.87 us: mechanism(): centre = gated - jnp.mean(gated, axis=-1, keepdims=True)]
  transfers between devices with their start and end apart: 4 -> 0, of which waited for: 4 -> 0; matrix products, arithmetic and copies ran while one was open for 25% -> 0% of each run, Pallas kernels for 0% -> 0%
where the time goes in v1:
time: 144 us; the launch traced here: 143 us
  Pallas kernels  130 us (90%)
  local copies, waits for them, and re-layouts  12.7 us (9%)
    pallas_call x1, Pallas kernels, on_device(): pl.pallas_call(kernel, out_shape=(jax.ShapeDtypeStruct(u_pre.shape, BF),...  130 us
    unnamed x19, local copies, waits for them, and re-layouts  12.7 us

profile of v1, /device:TPU:0, one launch (start us, length us, event | category | flops | bytes accessed | tf_op | source)
XLA Modules:
  0.0 143.1 jit_solution(1753955636907481539)
XLA Ops:
  0.6 129.6 %shard_map.135 = (bf16[1,1024,2048]{2,1,0:T(8,128)(2,1)}, bf16[1,1024,2048]{2,1,0:T(8,128)(2,1)}, f32[256,2048]{1,0:T(8,128)}, f32[16,128,128]{2,1,0:T(8,128)}, ...) custom-call(bf16[1,1024,2048]{2,1,0:T(8,128)(2,1)} %u_hbm.1, bf16[1,1024,2048]{2,1,0:T(8,128)(2,1)} %v_hbm.1, ...), custom_call_target="tpu_custom_call" | custom-call | tf_op jit(solution)/shard_map/pallas_call | solution.py:575
  130.3 0.0 copy-start
  130.3 4.9 %copy.22 = bf16[1,1024,2048]{2,1,0:T(8,128)(2,1)} copy(bf16[1,1024,2048]{2,1,0:T(8,128)(2,1)} %get-tuple-element.14) | data formatting | bytes 8388608
  135.2 0.0 copy-done
  135.2 0.0 copy-start.1
  135.2 2.1 %copy.23 = bf16[1,1024,2048]{2,1,0:T(8,128)(2,1)} copy(bf16[1,1024,2048]{2,1,0:T(8,128)(2,1)S(1)} %copy-done) | data formatting | bytes 8388608
  137.4 1.0 copy-done.1
  138.3 0.0 copy-start.2
  138.3 0.0 copy-start.5
  138.3 0.0 copy-start.4
  138.4 0.0 copy-start.3
  138.4 1.3 copy.24
  139.7 0.6 copy-done.2
  140.3 1.0 copy.25
  141.3 0.0 copy-done.5
  141.3 0.6 copy.26
  141.9 0.0 copy-done.4
  141.9 0.6 copy.27
  142.5 0.0 copy-done.3
  142.5 0.6 copy.28
Async XLA Ops:
  130.3 5.0 %copy-start = (bf16[1,1024,2048]{2,1,0:T(8,128)(2,1)S(1)}, bf16[1,1024,2048]{2,1,0:T(8,128)(2,1)}, u32[]{:S(2)}) copy-start(bf16[1,1024,2048]{2,1,0:T(8,128)(2,1)} %get-tuple-element.15) | copy-start | bytes 12582916
  135.2 3.1 %copy-start.1 = (f32[256,2048]{1,0:T(8,128)S(1)}, f32[256,2048]{1,0:T(8,128)}, u32[]{:S(2)}) copy-start(f32[256,2048]{1,0:T(8,128)} %get-tuple-element.16) | copy-start | bytes 6291460
  138.3 1.9 %copy-start.2 = (f32[16,128,128]{2,1,0:T(8,128)S(1)}, f32[16,128,128]{2,1,0:T(8,128)}, u32[]{:S(2)}) copy-start(f32[16,128,128]{2,1,0:T(8,128)} %get-tuple-element.17) | copy-start | bytes 3145732
  138.3 2.9 %copy-start.5 = (f32[16,128]{1,0:T(8,128)S(1)}, f32[16,128]{1,0:T(8,128)}, u32[]{:S(2)}) copy-start(f32[16,128]{1,0:T(8,128)} %get-tuple-element.18) | copy-start | bytes 24580
  138.3 3.5 %copy-start.4 = (f32[16,128]{1,0:T(8,128)S(1)}, f32[16,128]{1,0:T(8,128)}, u32[]{:S(2)}) copy-start(f32[16,128]{1,0:T(8,128)} %get-tuple-element.19) | copy-start | bytes 24580
  138.4 4.1 %copy-start.3 = (f32[16,128]{1,0:T(8,128)S(1)}, f32[16,128]{1,0:T(8,128)}, u32[]{:S(2)}) copy-start(f32[16,128]{1,0:T(8,128)} %get-tuple-element.20) | copy-start | bytes 24580

commit v2 on v1

v2 whole, which is shorter than its diff:
```python
import functools

import jax
import jax.numpy as jnp
from jax import lax
from jax.experimental import pallas as pl
from jax.experimental.pallas import tpu as pltpu
from jax.sharding import PartitionSpec as P

EPS = 1e-05
C0 = 0.7978845608028654
C1 = 0.044715
F32 = jnp.float32
BF = jnp.bfloat16
MESH = pl.DeviceIdType.MESH
WID = 2048
EXT = WID + 128


def rdma(src, dst, ssem, rsem, dev):
    return pltpu.make_async_remote_copy(
        src_ref=src, dst_ref=dst, send_sem=ssem, recv_sem=rsem, device_id=dev, device_id_type=MESH
    )


def al(v, m):
    return pl.multiple_of(v, m)


def gelu_pair(a):
    a2 = a * a
    th = jnp.tanh(a * (C0 + (C0 * C1) * a2))
    s = 0.5 + 0.5 * th
    g = a * s
    slope = s + g * (1.0 - s) * (2.0 * C0 + (6.0 * C0 * C1) * a2)
    return g, slope


def gelu_value(a):
    return a * (0.5 + 0.5 * jnp.tanh(a * (C0 + (C0 * C1) * (a * a))))


def gelu_slope(a):
    return gelu_pair(a)[1]


def lane_mean(a):
    return jnp.sum(a, axis=-1, keepdims=True) * (1.0 / 128.0)


def dot_nn(a, b):
    return lax.dot_general(a, b, (((1,), (0,)), ((), ())), preferred_element_type=F32)


def dot_nt(a, b):
    return lax.dot_general(a, b, (((1,), (1,)), ((), ())), preferred_element_type=F32)


def kernel(
    u_hbm, v_hbm, d_hbm, wm_hbm, bias_hbm, gain_hbm, shift_hbm, w_hbm,
    gu_ref, gv_ref, gw_ref, gm_ref, stat_ref,
    d_v, wbuf, ub, vb, gs, gt, pb, pr, tb, ra, rb, q, rc, rd, vx, rx, ob,
    qc, rc2, qd, rc3, cg, cp,
    st, st2, rs0, rs1, bias_ref, gain_ref, shift_ref, wl, wlt, bb, gwacc, bacc, gacc, sacc,
    sinv, sdn,
    ld_s, uv_s, wsend, wrecv, wrel_s, wrel_r,
    ps_s, ps_r, s1_s, s1_r, s2_s, s2_r, x_s, x_r, g1_s, g1_r, g2_s, g2_r,
    c_s, c_r, t_s, t_r,
):
    sp = lax.axis_index("sp")
    dp = lax.axis_index("dp")
    z, y = sp // 4, sp % 4
    x, c = dp // 2, dp % 2
    o = 1 - c

    def dev(x_, y_, z_, c_):
        return (z_ * 4 + y_, x_ * 2 + c_)

    def px(d):
        return dev((x + d) % 4, y, z, c)

    def py(d):
        return dev(x, (y + d) % 4, z, c)

    def pz(d):
        return dev(x, y, (z + d) % 4, c)

    mate = dev(x, y, z, o)
    first = (py, pz)
    second = (pz, py)
    i1 = (y, z)
    i2 = (z, y)

    own = [
        pltpu.make_async_copy(w_hbm.at[pl.ds(g * 128, 128)], wbuf.at[g, c], ld_s.at[g]) for g in range(2)
    ]
    dcp = [
        pltpu.make_async_copy(
            d_hbm.at[0, pl.ds(i * 256, 256)], d_v.at[pl.ds(i * 256, 256)], ld_s.at[2 + i]
        )
        for i in range(4)
    ]
    for cpy in own:
        cpy.start()
    params = [
        pltpu.make_async_copy(a, b, ld_s.at[6 + i])
        for i, (a, b) in enumerate(
            ((wm_hbm, wl), (bias_hbm, bias_ref), (gain_hbm, gain_ref), (shift_hbm, shift_ref))
        )
    ]
    for cpy in params:
        cpy.start()
    for cpy in dcp:
        cpy.start()

    def unit(u):
        par = u % 2
        quad = u // 2
        base = jnp.where(quad == 1, 3, jnp.where(quad == 2, 1, jnp.where(quad == 3, 2, 0)))
        xu = (x + base + par * quad * (3 - quad)) % 4
        return xu, par, quad

    def cols(u, cls):
        xu, par, _ = unit(u)
        return pl.ds(al((4 * xu + 2 * cls + par) * 128, 128), 128)

    def uv_copies(u):
        slot = u % 2
        res = []
        for k, (hbm, buf) in enumerate(((u_hbm, ub), (v_hbm, vb))):
            for cls in range(2):
                res.append(
                    pltpu.make_async_copy(
                        hbm.at[0, :, cols(u, cls)],
                        buf.at[slot, :, pl.ds(cls * 128, 128)],
                        uv_s.at[slot, k, cls],
                    )
                )
        return res

    for cpy in uv_copies(0):
        cpy.start()

    barrier = pltpu.get_barrier_semaphore()
    for peer in [mate] + [f(d) for f in (px, py, pz) for d in (1, 2, 3)]:
        pl.semaphore_signal(barrier, inc=1, device_id=peer, device_id_type=MESH)
    pl.semaphore_wait(barrier, 10)

    def wx(k):
        src, dst, d = ((0, 2, 1), (1, 3, 3), (1, 5, 1), (0, 4, 3), (2, 6, 1), (3, 7, 3))[k]
        return rdma(wbuf.at[src, c], wbuf.at[dst, c], wsend.at[k], wrecv.at[k], px(d))

    arrival = {2: 0, 3: 1, 5: 2, 4: 3, 6: 4, 7: 5}

    def relay(s, k):
        return rdma(wbuf.at[s, k], wbuf.at[s, k], wrel_s.at[s], wrel_r.at[s], mate)

    for cpy in own:
        cpy.wait()
    relay(0, c).start()
    relay(1, c).start()
    for k in range(4):
        wx(k).start()

    tri = lax.broadcasted_iota(jnp.int32, (128, 128), 0) >= lax.broadcasted_iota(jnp.int32, (128, 128), 1)

    def prep(g, _):
        w = jnp.where(tri, wl[g].astype(F32), 0.0)
        wl[g] = w.astype(BF)
        wlt[g] = w.T.astype(BF)
        return 0

    for cpy in params:
        cpy.wait()
    lax.fori_loop(0, 16, prep, 0)
    for cpy in dcp:
        cpy.wait()

    def ps(u):
        return rdma(pb.at[u % 2, o], pr.at[u % 2], ps_s.at[u % 2], ps_r.at[u], mate)

    WAB = (1152, 1024)
    OFF = (0, 1152)

    def rows(j, half=None):
        if half is None:
            return pl.ds(al(32 * j, 32), 32)
        return pl.ds(al(32 * j + 16 * half, 16), 16)

    def lanes(j):
        return pl.ds(al(256 * j, 256), 256)

    HOP = (1, 3)

    def s1a(u, ab, k):
        w = WAB[ab]
        return rdma(
            tb.at[u % 4, rows((i1[ab] + 2) % 4, k), pl.ds(OFF[ab], w)],
            ra.at[u, ab, k, :, pl.ds(0, w)],
            s1_s.at[u % 4, 0, ab, k], s1_r.at[u, 0, ab, k], first[ab](HOP[k]),
        )

    def s1b(u, ab, k):
        w = WAB[ab]
        return rdma(
            tb.at[u % 4, rows((i1[ab] + HOP[k]) % 4), pl.ds(OFF[ab], w)],
            rb.at[u, ab, k, :, pl.ds(0, w)],
            s1_s.at[u % 4, 1, ab, k], s1_r.at[u, 1, ab, k], first[ab](HOP[k]),
        )

    def s2a(u, ab, k):
        return rdma(
            q.at[u % 4, ab, pl.ds(16 * k, 16), lanes((i2[ab] + 2) % 4)],
            rc.at[u, ab, k],
            s2_s.at[u % 4, 0, ab, k], s2_r.at[u, 0, ab, k], second[ab](HOP[k]),
        )

    def s2b(u, ab, k):
        return rdma(
            q.at[u % 4, ab, :, lanes((i2[ab] + HOP[k]) % 4)],
            rd.at[u, ab, k],
            s2_s.at[u % 4, 1, ab, k], s2_r.at[u, 1, ab, k], second[ab](HOP[k]),
        )

    def xs(u):
        xu, par, quad = unit(u)
        return rdma(vx.at[u], rx.at[par, quad], x_s.at[u], x_r.at[par, quad], dev(xu, y, z, c))

    PAIRS = [(ab, d) for ab in range(2) for d in (1, 2, 3)]
    BOTH = [(ab, k) for ab in range(2) for k in range(2)]

    def do_ts(u):
        ps(u).wait()
        slot = u % 4

        def body(i, _):
            r = pl.ds(al(i * 16, 16), 16)
            for src, dst, w in ((0, 0, 1024), (WID, 1024, 128), (1024, 1152, 1024)):
                tb[slot, r, pl.ds(dst, w)] = (
                    pb[u % 2, c, r, pl.ds(src, w)].astype(F32) + pr[u % 2, r, pl.ds(src, w)].astype(F32)
                ).astype(BF)
            return 0

        lax.fori_loop(0, 8, body, 0)
        for ab, k in BOTH:
            s1a(u, ab, k).start()

    def do_s1b(u):
        slot = u % 4
        for ab, k in BOTH:
            s1a(u, ab, k).wait_recv()
        for ab, k in BOTH:
            r, ln = rows((i1[ab] + HOP[k]) % 4, k), pl.ds(OFF[ab], WAB[ab])
            tb[slot, r, ln] = (
                tb[slot, r, ln].astype(F32) + ra[u, ab, k, :, pl.ds(0, WAB[ab])].astype(F32)
            ).astype(BF)
        for ab, k in BOTH:
            s1b(u, ab, k).start()

    def do_s2a(u):
        slot = u % 4
        xu, par, _ = unit(u)
        for ab, k in BOTH:
            s1a(u, ab, k).wait_send()
            s1b(u, ab, k).wait()
        for ab in range(2):
            for h in range(2):
                hs = pl.ds(16 * h, 16)

                def total(a, w):
                    acc = tb[slot, rows(i1[ab], h), pl.ds(OFF[ab] + a, w)].astype(F32)
                    for k in range(2):
                        acc = acc + rb[u, ab, k, hs, pl.ds(a, w)].astype(F32)
                    return acc.astype(BF)

                q[slot, ab, hs, :] = total(0, 1024)
                if ab == 0:
                    qc[xu * 2 + par, hs, :] = total(1024, 128)
        for ab, k in BOTH:
            s2a(u, ab, k).start()

    def do_s2b(u):
        slot = u % 4
        for ab, k in BOTH:
            s2a(u, ab, k).wait_recv()
        for ab, k in BOTH:
            hs, ln = pl.ds(16 * k, 16), lanes((i2[ab] + HOP[k]) % 4)
            q[slot, ab, hs, ln] = (q[slot, ab, hs, ln].astype(F32) + rc[u, ab, k].astype(F32)).astype(BF)
        for ab, k in BOTH:
            s2b(u, ab, k).start()

    def do_x(u):
        slot = u % 4
        for ab, k in BOTH:
            s2a(u, ab, k).wait_send()
            s2b(u, ab, k).wait()
        for ab in range(2):
            acc = q[slot, ab, :, lanes(i2[ab])].astype(F32)
            for k in range(2):
                acc = acc + rd[u, ab, k].astype(F32)
            vx[u, ab] = acc.astype(BF)

        @pl.when(u >= 2)
        def _():
            xs(u).start()

    def ob_small(g, ab, j):
        return ob.at[
            pl.ds(al(g * 128 + 32 * i1[ab], 32), 32), pl.ds(al(1024 * ab + 256 * j, 256), 256)
        ]

    def ob_big(g, ab, j, half=None):
        r = pl.ds(al(g * 128 + 32 * j, 32), 32)
        if half is not None:
            r = pl.ds(al(g * 128 + 32 * j + 16 * half, 16), 16)
        return ob.at[r, pl.ds(1024 * ab, 1024)]

    def g1(g, ab, d, j):
        return rdma(
            ob_small(g, ab, j), ob_small(g, ab, j), g1_s.at[g, ab, d - 1], g1_r.at[g, ab, d - 1], second[ab](d)
        )

    def g2a(g, ab, k, j):
        return rdma(
            ob_big(g, ab, j), ob_big(g, ab, j),
            g2_s.at[g, 0, ab, k], g2_r.at[g, 0, ab, k], first[ab](HOP[k]),
        )

    def g2b(g, ab, k, j):
        ref = ob_big(g, ab, j, k)
        return rdma(ref, ref, g2_s.at[g, 1, ab, k], g2_r.at[g, 1, ab, k], first[ab](HOP[k]))

    def do_f(g):
        for k in (1, 2, 3):
            rdma(vx.at[g], rx.at[g, k], x_s.at[g], x_r.at[g, k], mate).wait_recv()
        for ab in range(2):
            acc = vx[g, ab].astype(F32)
            for k in (1, 2, 3):
                acc = acc + rx[g, k, ab].astype(F32)
            ob_small(g, ab, i2[ab])[...] = acc.astype(BF)
        for ab, d in PAIRS:
            g1(g, ab, d, i2[ab]).start()

    def do_g2a(g):
        for ab, d in PAIRS:
            g1(g, ab, d, (i2[ab] + 4 - d) % 4).wait_recv()
        for ab, k in BOTH:
            g2a(g, ab, k, i1[ab]).start()

    def do_g2b(g):
        for ab, k in BOTH:
            g2a(g, ab, k, (i1[ab] + HOP[1 - k]) % 4).wait_recv()
        for ab, k in BOTH:
            g2b(g, ab, k, (i1[ab] + HOP[1 - k]) % 4).start()

    def do_out(g):
        for ab, k in BOTH:
            g2b(g, ab, k, (i1[ab] + 2) % 4).wait_recv()

        def body(i, _):
            r = pl.ds(al(g * 128 + i * 16, 16), 16)
            gw_ref[r, :] = ob[r, :].astype(F32)
            return 0

        lax.fori_loop(0, 8, body, 0)

    def arrive(s):
        wx(arrival[s]).wait_recv()
        relay(s, c).start()

    def unit_body(u, _):
        slot = u % 2
        xu, par, _q = unit(u)
        relay(u, o).wait_recv()

        @pl.when(u < 7)
        def _():
            for cpy in uv_copies(u + 1):
                cpy.start()

        gs[...] = dot_nt(d_v[...], wbuf[u].reshape(256, WID)).astype(BF)

        for cpy in uv_copies(u):
            cpy.wait()

        for cls in range(2):
            row = bias_ref[pl.ds(4 * xu + 2 * cls + par, 1), :]
            bb[cls] = jnp.broadcast_to(row, (128, 128)).T
        gwacc[...] = jnp.zeros_like(gwacc)
        bacc[...] = jnp.zeros_like(bacc)
        gacc[...] = jnp.zeros_like(gacc)
        sacc[...] = jnp.zeros_like(sacc)

        def block(n, _):
            r = pl.ds(al(n * 128, 128), 128)
            for cls in range(2):
                grp = 4 * xu + 2 * cls + par
                ln = pl.ds(cls * 128, 128)
                gain = gain_ref[pl.ds(grp, 1), :]
                shift = shift_ref[pl.ds(grp, 1), :]
                gated = gelu_value(vb[slot, r, ln].astype(F32))
                cen = gated - lane_mean(gated)
                inv = lax.rsqrt(lane_mean(cen * cen) + EPS)
                scaled = cen * inv
                gv_ref[0, r, cols(u, cls)] = scaled.astype(BF)
                sinv[u, r, ln] = jnp.broadcast_to(inv, (128, 128)).astype(BF)
                nb = (scaled * gain + shift).astype(BF)
                upper, u_slope = gelu_pair(ub[slot, r, ln].astype(F32))
                cot = gs[r, ln].astype(F32)
                dm = cot * upper
                dmb = dm.astype(BF)
                bacc[cls] += dm
                mixed = dot_nn(wl[grp], nb) + bb[cls]
                dn = dot_nn(wlt[grp], dmb)
                gwacc[cls] += dot_nt(dmb, nb)
                gt[pl.ds(cls * 128, 128), r] = (upper * mixed).T.astype(BF)
                gu_ref[0, r, cols(u, cls)] = (cot * mixed * u_slope).astype(BF)
                prod = dn * scaled
                gacc[cls] += jnp.sum(prod.reshape(16, 8, 128), axis=0)
                sacc[cls] += jnp.sum(dn.reshape(16, 8, 128), axis=0)
                sdn[u, r, ln] = dn.astype(BF)
            return 0

        lax.fori_loop(0, 8, block, 0, unroll=4)

        for lag, act in ((5, do_x), (4, do_s2b), (3, do_s2a), (2, do_s1b), (1, do_ts)):

            @pl.when(u >= lag)
            def _(lag=lag, act=act):
                act(u - lag)

        pb[slot, :, :, pl.ds(0, WID)] = dot_nn(gt[...], d_v[...]).astype(BF).reshape(2, 128, WID)
        for cls in range(2):
            grp = 4 * xu + 2 * cls + par
            pb[slot, cls, :, pl.ds(WID, 128)] = jnp.where(tri, gwacc[cls], 0.0).astype(BF)
            st[0, pl.ds(grp, 1), :] = jnp.sum(bacc[cls].T, axis=0, keepdims=True)
            st[1, pl.ds(grp, 1), :] = jnp.sum(gacc[cls], axis=0, keepdims=True)
            st[2, pl.ds(grp, 1), :] = jnp.sum(sacc[cls], axis=0, keepdims=True)
        ps(u).start()

        @pl.when(u == 1)
        def _():
            arrive(2)
            wx(4).start()
            arrive(3)
            wx(5).start()

        @pl.when(u == 3)
        def _():
            arrive(4)
            arrive(5)

        @pl.when(u == 5)
        def _():
            arrive(6)
            arrive(7)

        return 0

    lax.fori_loop(0, 8, unit_body, 0)

    def v_copies(u):
        return uv_copies(u)[2:]

    def finish(u):
        slot = u % 2
        xu, par, _ = unit(u)
        for cpy in v_copies(u):
            cpy.wait()
        if u < 7:
            for cpy in v_copies(u + 1):
                cpy.start()

        def block(n, _):
            r = pl.ds(al(n * 128, 128), 128)
            for cls in range(2):
                ln = pl.ds(cls * 128, 128)
                gain = gain_ref[pl.ds(4 * xu + 2 * cls + par, 1), :]
                slope = gelu_slope(vb[slot, r, ln].astype(F32))
                scaled = gv_ref[0, r, cols(u, cls)].astype(F32)
                e = sdn[u, r, ln].astype(F32) * gain
                m1 = lane_mean(e)
                m2 = lane_mean(e * scaled)
                gv_ref[0, r, cols(u, cls)] = (
                    (e - m1 - scaled * m2) * (slope * sinv[u, r, ln].astype(F32))
                ).astype(BF)
            return 0

        lax.fori_loop(0, 8, block, 0, unroll=4)

    for cpy in v_copies(0):
        cpy.start()

    def stat_sum(src, parts, dst):
        acc = src[...]
        for part in parts:
            acc = acc + part[...]
        dst[...] = acc

    t0 = rdma(st, rs0, t_s.at[0, 0], t_r.at[0, 0], mate)
    t0.start()

    def tstage(k, d, src, f):
        return rdma(src, rs1.at[k, d - 1], t_s.at[k + 1, d - 1], t_r.at[k + 1, d - 1], f(d))

    def cz(d, j):
        return rdma(qc.at[pl.ds(2 * j, 2)], rc2.at[d - 1], c_s.at[1, d - 1], c_r.at[1, d - 1], pz(d))

    def cx(d):
        return rdma(qd, rc3.at[d - 1], c_s.at[2, d - 1], c_r.at[2, d - 1], px(d))

    def cgz(d, j):
        ref = cg.at[pl.ds(2 * j, 2), pl.ds(al(32 * y, 32), 32)]
        return rdma(ref, ref, c_s.at[3, d - 1], c_r.at[3, d - 1], pz(d))

    def cga(k, j):
        ref = cg.at[:, pl.ds(al(32 * j, 32), 32)]
        return rdma(ref, ref, c_s.at[4, k], c_r.at[4, k], py(HOP[k]))

    def cgb(k, j):
        ref = cg.at[pl.ds(4 * k, 4), pl.ds(al(32 * j, 32), 32)]
        return rdma(ref, ref, c_s.at[0, k], c_r.at[0, k], py(HOP[k]))

    DS = (1, 2, 3)

    def pipe(n):
        for lag, act in ((5, do_x), (4, do_s2b), (3, do_s2a), (2, do_s1b), (1, do_ts)):
            if 0 <= n - lag <= 7:
                act(n - lag)

    def stat_step(k, f, g):
        for d in DS:
            tstage(k, d, st2.at[k], f).wait()
        if k < 2:
            stat_sum(st2.at[k], [rs1.at[k, i] for i in range(3)], st2.at[k + 1])
            for d in DS:
                tstage(k + 1, d, st2.at[k + 1], g).start()

    finish(0)
    pipe(8)
    t0.wait()
    stat_sum(st, [rs0], st2.at[0])
    for d in DS:
        tstage(0, d, st2.at[0], py).start()
    finish(1)
    pipe(9)
    stat_step(0, py, pz)
    finish(2)
    pipe(10)
    for d in DS:
        cz(d, (z + d) % 4).start()
    stat_step(1, pz, px)
    finish(3)
    pipe(11)
    for d in DS:
        cz(d, (z + d) % 4).wait()
    acc = qc[pl.ds(2 * z, 2)].astype(F32)
    for k in range(3):
        acc = acc + rc2[k].astype(F32)
    qd[...] = acc.astype(BF)
    for d in DS:
        cx(d).start()
    finish(4)
    pipe(12)
    do_f(0)
    for d in DS:
        cx(d).wait()
    acc = qd[...].astype(F32)
    for k in range(3):
        acc = acc + rc3[k].astype(F32)
    cg[pl.ds(2 * z, 2), pl.ds(al(32 * y, 32), 32), :] = acc.astype(BF)
    for d in DS:
        cgz(d, z).start()
    stat_step(2, px, None)
    tot = st2[2]
    for k in range(3):
        tot = tot + rs1[2, k]
    stat_ref[...] = tot
    finish(5)
    do_f(1)
    do_g2a(0)
    for d in DS:
        cgz(d, (z + 4 - d) % 4).wait_recv()
    for k in range(2):
        cga(k, y).start()
    finish(6)
    do_g2a(1)
    do_g2b(0)
    for k in range(2):
        cga(k, (y + HOP[1 - k]) % 4).wait_recv()
    for k in range(2):
        cgb(k, (y + HOP[1 - k]) % 4).start()
    finish(7)
    do_g2b(1)
    for k in range(2):
        cgb(k, (y + 2) % 4).wait_recv()
    swap = rdma(cg, cp, c_s.at[5, 0], c_r.at[5, 0], mate)
    swap.start()
    do_out(0)

    def gm_body(src, cls):
        def body(i, _):
            gm_ref[(i // 2) * 4 + 2 * cls + i % 2] = src[i].astype(F32)
            return 0

        lax.fori_loop(0, 8, body, 0)

    gm_body(cg, c)
    do_out(1)
    swap.wait()
    gm_body(cp, o)

    for k in range(6):
        wx(k).wait_send()
    for s in range(8):
        relay(s, c).wait_send()
    for u in range(2, 8):
        xs(u).wait_send()
    for g in range(2):
        for ab, d in PAIRS:
            g1(g, ab, d, i2[ab]).wait_send()
        for ab, k in BOTH:
            g2a(g, ab, k, i1[ab]).wait_send()
            g2b(g, ab, k, (i1[ab] + HOP[1 - k]) % 4).wait_send()
    for d in DS:
        cgz(d, z).wait_send()
    for k in range(2):
        cga(k, y).wait_send()
        cgb(k, (y + HOP[1 - k]) % 4).wait_send()


def place(gu, gv, gw, gm, st, o_gu, o_gv, o_gw, o_gm, o_b, o_g, o_s, sem):
    moves = [(gu, o_gu), (gv, o_gv), (gw, o_gw), (gm, o_gm), (st.at[0], o_b), (st.at[1], o_g), (st.at[2], o_s)]
    cps = [pltpu.make_async_copy(a, b, sem.at[i]) for i, (a, b) in enumerate(moves)]
    for cpy in cps:
        cpy.start()
    for cpy in cps:
        cpy.wait()


def on_device(u_pre, v_pre, d_out, w_mix, mix_bias, norm_gain, norm_shift, w_out):
    hbm = pl.BlockSpec(memory_space=pltpu.HBM)
    vm = pl.BlockSpec(memory_space=pltpu.VMEM)
    V = pltpu.VMEM
    DMA = pltpu.SemaphoreType.DMA
    scratch = [
        V((1024, WID), BF), V((8, 2, 128, WID), BF),
        V((2, 1024, 256), BF), V((2, 1024, 256), BF),
        V((1024, 256), BF), V((256, 1024), BF),
        V((2, 2, 128, EXT), BF), V((2, 128, EXT), BF), V((4, 128, EXT), BF),
        V((8, 2, 2, 16, 1152), BF), V((8, 2, 2, 32, 1152), BF), V((4, 2, 32, 1024), BF),
        V((8, 2, 2, 16, 256), BF), V((8, 2, 2, 32, 256), BF),
        V((8, 2, 32, 256), BF), V((2, 4, 2, 32, 256), BF), V((256, WID), BF),
        V((8, 32, 128), BF), V((3, 2, 32, 128), BF),
        V((2, 32, 128), BF), V((3, 2, 32, 128), BF), V((8, 128, 128), BF), V((8, 128, 128), BF),
        V((3, 16, 128), F32), V((3, 3, 16, 128), F32), V((3, 16, 128), F32), V((3, 3, 3, 16, 128), F32),
        V((16, 128), F32), V((16, 128), F32), V((16, 128), F32),
        V((16, 128, 128), BF), V((16, 128, 128), BF), V((2, 128, 128), F32),
        V((2, 128, 128), F32), V((2, 128, 128), F32), V((2, 8, 128), F32), V((2, 8, 128), F32),
        V((8, 1024, 256), BF), V((8, 1024, 256), BF),
        DMA((10,)), DMA((2, 2, 2)), DMA((6,)), DMA((6,)), DMA((8,)), DMA((8,)),
        DMA((2,)), DMA((8,)), DMA((4, 2, 2, 2)), DMA((8, 2, 2, 2)), DMA((4, 2, 2, 2)), DMA((8, 2, 2, 2)),
        DMA((8,)), DMA((2, 4)), DMA((2, 2, 3)), DMA((2, 2, 3)), DMA((2, 2, 2, 2)), DMA((2, 2, 2, 2)),
        DMA((6, 3)), DMA((6, 3)), DMA((4, 3)), DMA((4, 3)),
    ]
    outs = pl.pallas_call(
        kernel,
        out_shape=(
            jax.ShapeDtypeStruct(u_pre.shape, BF),
            jax.ShapeDtypeStruct(v_pre.shape, BF),
            jax.ShapeDtypeStruct((256, WID), F32),
            jax.ShapeDtypeStruct((16, 128, 128), F32),
            jax.ShapeDtypeStruct((3, 16, 128), F32),
        ),
        in_specs=[hbm] * 8,
        out_specs=(vm, vm, vm, vm, vm),
        scratch_shapes=scratch,
        compiler_params=pltpu.CompilerParams(
            collective_id=0, has_side_effects=True, vmem_limit_bytes=39 * 1024 * 1024
        ),
    )(u_pre, v_pre, d_out, w_mix, mix_bias, norm_gain, norm_shift, w_out)
    anyspace = pl.BlockSpec(memory_space=pl.ANY)
    small = jax.ShapeDtypeStruct((16, 128), F32)
    return pl.pallas_call(
        place,
        out_shape=(
            jax.ShapeDtypeStruct(u_pre.shape, BF),
            jax.ShapeDtypeStruct(v_pre.shape, BF),
            jax.ShapeDtypeStruct((256, WID), F32),
            jax.ShapeDtypeStruct((16, 128, 128), F32),
            small, small, small,
        ),
        in_specs=[anyspace] * 5,
        out_specs=(hbm,) * 7,
        scratch_shapes=[DMA((7,))],
        compiler_params=pltpu.CompilerParams(vmem_limit_bytes=512 * 1024),
    )(*outs)


def solution(mesh):
    return jax.shard_map(
        on_device,
        mesh=mesh,
        in_specs=(
            P("dp", "sp", None), P("dp", "sp", None), P("dp", "sp", None),
            P(), P(), P(), P(), P("dp", None),
        ),
        out_specs=(P("dp", "sp", None), P("dp", "sp", None), P("dp", None), P(), P(), P(), P()),
        check_vma=False,
    )
```

time: 144 us -> 107 us (0.74)
  Pallas kernels: 130 us -> 102 us
  local copies, waits for them, and re-layouts: 12.7 us -> 4.35 us
    pallas_call x1, Pallas kernels: 130 us -> 97.3 us  [on_device(): pl.pallas_call(kernel, out_shape=(jax.ShapeDtypeStruct(u_pre.shape, BF),...]
    unnamed x19 -> x10, local copies, waits for them, and re-layouts: 12.7 us -> 4.35 us
    pallas_call x0 -> x1, Pallas kernels: none -> 4.31 us  [on_device(): pl.pallas_call(place, out_shape=(jax.ShapeDtypeStruct(u_pre.shape, BF), j...]
where the time goes in v2:
time: 107 us
  Pallas kernels  102 us (95%)
  local copies, waits for them, and re-layouts  4.35 us (4%)
    pallas_call x1, Pallas kernels, on_device(): pl.pallas_call(kernel, out_shape=(jax.ShapeDtypeStruct(u_pre.shape, BF),...  97.3 us
    unnamed x10, local copies, waits for them, and re-layouts  4.35 us
    pallas_call x1, Pallas kernels, on_device(): pl.pallas_call(place, out_shape=(jax.ShapeDtypeStruct(u_pre.shape, BF), j...  4.31 us

profile of v2, /device:TPU:0, one launch (start us, length us, event | category | flops | bytes accessed | tf_op | source)
XLA Modules:
  0.0 106.6 jit_solution(11425062125506441790)
XLA Ops:
  0.6 0.0 copy-start
  0.6 1.2 %copy-done = bf16[256,2048]{1,0:T(8,128)(2,1)S(1)} copy-done((bf16[256,2048]{1,0:T(8,128)(2,1)S(1)}, bf16[256,2048]{1,0:T(8,128)(2,1)}, u32[]{:S(2)}) %copy-start) | copy-done | bytes 1048600
  1.9 0.0 copy-start.1
  1.9 1.0 copy-done.1
  2.9 0.0 copy-start.2
  2.9 0.7 copy-done.2
  3.6 0.0 copy-start.3
  3.6 0.7 copy-done.3
  4.3 0.0 copy-start.4
  4.3 0.7 copy-done.4
  5.0 97.3 %shard_map.135 = (bf16[1,1024,2048]{2,1,0:T(8,128)(2,1)S(1)}, bf16[1,1024,2048]{2,1,0:T(8,128)(2,1)S(1)}, f32[256,2048]{1,0:T(8,128)S(1)}, f32[16,128,128]{2,1,0:T(8,128)S(1)}, f32[3,16,128]{2,1,0:T(8,128)S(1)}) custom-call(bf16[1,1024,2048]{2,1,0:T(8,128)(2,1)} %u_hbm.1, bf16[1,1024,2048]{2,1,0:T(8,128)(2,1)} %v_hbm.1, bf16[1,1024,2048]{2,1,0:T(8,128)(2,1)} %d_hbm.1, ...), custom_call_target="tpu_custom_call" | custom-call | tf_op jit(solution)/shard_map/pallas_call | solution.py:666
  102.3 4.3 %shard_map.136 = (bf16[1,1024,2048]{2,1,0:T(8,128)(2,1)}, bf16[1,1024,2048]{2,1,0:T(8,128)(2,1)}, f32[256,2048]{1,0:T(8,128)}, f32[16,128,128]{2,1,0:T(8,128)}, ...) custom-call(bf16[1,1024,2048]{2,1,0:T(8,128)(2,1)S(1)} %get-tuple-element.12.gu, ...), custom_call_target="tpu_custom_call" | custom-call | tf_op jit(solution)/shard_map/pallas_call | solution.py:684
Async XLA Ops:
  0.6 1.2 %copy-start = (bf16[256,2048]{1,0:T(8,128)(2,1)S(1)}, bf16[256,2048]{1,0:T(8,128)(2,1)}, u32[]{:S(2)}) copy-start(bf16[256,2048]{1,0:T(8,128)(2,1)} %w_hbm.1) | copy-start | bytes 3145732
  1.9 1.0 copy-start.1
  2.9 0.7 copy-start.2
  3.6 0.7 copy-start.3
  4.3 0.7 copy-start.4

commit v3 on v2

--- a/solution.py
+++ b/solution.py
@@ -113,16 +113,18 @@
     for cpy in dcp:
         cpy.start()
 
-    def unit(u):
+    def unit(u, cls):
         par = u % 2
         quad = u // 2
-        base = jnp.where(quad == 1, 3, jnp.where(quad == 2, 1, jnp.where(quad == 3, 2, 0)))
-        xu = (x + base + par * quad * (3 - quad)) % 4
+        xu = (x + jnp.where(cls == 0, 4 - quad, quad)) % 4
         return xu, par, quad
 
+    def group(u, cls):
+        xu, par, _ = unit(u, cls)
+        return 4 * xu + 2 * cls + par
+
     def cols(u, cls):
-        xu, par, _ = unit(u)
-        return pl.ds(al((4 * xu + 2 * cls + par) * 128, 128), 128)
+        return pl.ds(al(group(u, cls) * 128, 128), 128)
 
     def uv_copies(u):
         slot = u % 2
@@ -147,10 +149,7 @@
     pl.semaphore_wait(barrier, 10)
 
     def wx(k):
-        src, dst, d = ((0, 2, 1), (1, 3, 3), (1, 5, 1), (0, 4, 3), (2, 6, 1), (3, 7, 3))[k]
-        return rdma(wbuf.at[src, c], wbuf.at[dst, c], wsend.at[k], wrecv.at[k], px(d))
-
-    arrival = {2: 0, 3: 1, 5: 2, 4: 3, 6: 4, 7: 5}
+        return rdma(wbuf.at[k, c], wbuf.at[k + 2, c], wsend.at[k], wrecv.at[k], px(1 + 2 * c))
 
     def relay(s, k):
         return rdma(wbuf.at[s, k], wbuf.at[s, k], wrel_s.at[s], wrel_r.at[s], mate)
@@ -159,7 +158,7 @@
         cpy.wait()
     relay(0, c).start()
     relay(1, c).start()
-    for k in range(4):
+    for k in range(2):
         wx(k).start()
 
     tri = lax.broadcasted_iota(jnp.int32, (128, 128), 0) >= lax.broadcasted_iota(jnp.int32, (128, 128), 1)
@@ -223,7 +222,7 @@
         )
 
     def xs(u):
-        xu, par, quad = unit(u)
+        xu, par, quad = unit(u, c)
         return rdma(vx.at[u], rx.at[par, quad], x_s.at[u], x_r.at[par, quad], dev(xu, y, z, c))
 
     PAIRS = [(ab, d) for ab in range(2) for d in (1, 2, 3)]
@@ -236,9 +235,7 @@
         def body(i, _):
             r = pl.ds(al(i * 16, 16), 16)
             for src, dst, w in ((0, 0, 1024), (WID, 1024, 128), (1024, 1152, 1024)):
-                tb[slot, r, pl.ds(dst, w)] = (
-                    pb[u % 2, c, r, pl.ds(src, w)].astype(F32) + pr[u % 2, r, pl.ds(src, w)].astype(F32)
-                ).astype(BF)
+                tb[slot, r, pl.ds(dst, w)] = pb[u % 2, c, r, pl.ds(src, w)] + pr[u % 2, r, pl.ds(src, w)]
             return 0
 
         lax.fori_loop(0, 8, body, 0)
@@ -251,15 +248,13 @@
             s1a(u, ab, k).wait_recv()
         for ab, k in BOTH:
             r, ln = rows((i1[ab] + HOP[k]) % 4, k), pl.ds(OFF[ab], WAB[ab])
-            tb[slot, r, ln] = (
-                tb[slot, r, ln].astype(F32) + ra[u, ab, k, :, pl.ds(0, WAB[ab])].astype(F32)
-            ).astype(BF)
+            tb[slot, r, ln] = tb[slot, r, ln] + ra[u, ab, k, :, pl.ds(0, WAB[ab])]
         for ab, k in BOTH:
             s1b(u, ab, k).start()
 
     def do_s2a(u):
         slot = u % 4
-        xu, par, _ = unit(u)
+        xu, par, _ = unit(u, c)
         for ab, k in BOTH:
             s1a(u, ab, k).wait_send()
             s1b(u, ab, k).wait()
@@ -285,7 +280,7 @@
             s2a(u, ab, k).wait_recv()
         for ab, k in BOTH:
             hs, ln = pl.ds(16 * k, 16), lanes((i2[ab] + HOP[k]) % 4)
-            q[slot, ab, hs, ln] = (q[slot, ab, hs, ln].astype(F32) + rc[u, ab, k].astype(F32)).astype(BF)
+            q[slot, ab, hs, ln] = q[slot, ab, hs, ln] + rc[u, ab, k]
         for ab, k in BOTH:
             s2b(u, ab, k).start()
 
@@ -365,12 +360,15 @@
         lax.fori_loop(0, 8, body, 0)
 
     def arrive(s):
-        wx(arrival[s]).wait_recv()
+        wx(s - 2).wait_recv()
         relay(s, c).start()
+
+        @pl.when(s < 6)
+        def _():
+            wx(s).start()
 
     def unit_body(u, _):
         slot = u % 2
-        xu, par, _q = unit(u)
         relay(u, o).wait_recv()
 
         @pl.when(u < 7)
@@ -380,11 +378,16 @@
 
         gs[...] = dot_nt(d_v[...], wbuf[u].reshape(256, WID)).astype(BF)
 
+        @pl.when((u >= 1) & (u < 7))
+        def _():
+            arrive(u + 1)
+
+
         for cpy in uv_copies(u):
             cpy.wait()
 
         for cls in range(2):
-            row = bias_ref[pl.ds(4 * xu + 2 * cls + par, 1), :]
+            row = bias_ref[pl.ds(group(u, cls), 1), :]
             bb[cls] = jnp.broadcast_to(row, (128, 128)).T
         gwacc[...] = jnp.zeros_like(gwacc)
         bacc[...] = jnp.zeros_like(bacc)
@@ -394,7 +397,7 @@
         def block(n, _):
             r = pl.ds(al(n * 128, 128), 128)
             for cls in range(2):
-                grp = 4 * xu + 2 * cls + par
+                grp = group(u, cls)
                 ln = pl.ds(cls * 128, 128)
                 gain = gain_ref[pl.ds(grp, 1), :]
                 shift = shift_ref[pl.ds(grp, 1), :]
@@ -405,7 +408,7 @@
                 gv_ref[0, r, cols(u, cls)] = scaled.astype(BF)
                 sinv[u, r, ln] = jnp.broadcast_to(inv, (128, 128)).astype(BF)
                 nb = (scaled * gain + shift).astype(BF)
-                upper, u_slope = gelu_pair(ub[slot, r, ln].astype(F32))
+                upper = gelu_value(ub[slot, r, ln].astype(F32))
                 cot = gs[r, ln].astype(F32)
                 dm = cot * upper
                 dmb = dm.astype(BF)
@@ -414,7 +417,7 @@
                 dn = dot_nn(wlt[grp], dmb)
                 gwacc[cls] += dot_nt(dmb, nb)
                 gt[pl.ds(cls * 128, 128), r] = (upper * mixed).T.astype(BF)
-                gu_ref[0, r, cols(u, cls)] = (cot * mixed * u_slope).astype(BF)
+                gu_ref[0, r, cols(u, cls)] = (cot * mixed).astype(BF)
                 prod = dn * scaled
                 gacc[cls] += jnp.sum(prod.reshape(16, 8, 128), axis=0)
                 sacc[cls] += jnp.sum(dn.reshape(16, 8, 128), axis=0)
@@ -431,40 +434,22 @@
 
         pb[slot, :, :, pl.ds(0, WID)] = dot_nn(gt[...], d_v[...]).astype(BF).reshape(2, 128, WID)
         for cls in range(2):
-            grp = 4 * xu + 2 * cls + par
+            grp = group(u, cls)
             pb[slot, cls, :, pl.ds(WID, 128)] = jnp.where(tri, gwacc[cls], 0.0).astype(BF)
             st[0, pl.ds(grp, 1), :] = jnp.sum(bacc[cls].T, axis=0, keepdims=True)
             st[1, pl.ds(grp, 1), :] = jnp.sum(gacc[cls], axis=0, keepdims=True)
             st[2, pl.ds(grp, 1), :] = jnp.sum(sacc[cls], axis=0, keepdims=True)
         ps(u).start()
 
-        @pl.when(u == 1)
-        def _():
-            arrive(2)
-            wx(4).start()
-            arrive(3)
-            wx(5).start()
-
-        @pl.when(u == 3)
-        def _():
-            arrive(4)
-            arrive(5)
-
-        @pl.when(u == 5)
-        def _():
-            arrive(6)
-            arrive(7)
-
         return 0
 
     lax.fori_loop(0, 8, unit_body, 0)
 
     def v_copies(u):
-        return uv_copies(u)[2:]
+        return uv_copies(u)
 
     def finish(u):
         slot = u % 2
-        xu, par, _ = unit(u)
         for cpy in v_copies(u):
             cpy.wait()
         if u < 7:
@@ -475,7 +460,11 @@
             r = pl.ds(al(n * 128, 128), 128)
             for cls in range(2):
                 ln = pl.ds(cls * 128, 128)
-                gain = gain_ref[pl.ds(4 * xu + 2 * cls + par, 1), :]
+                gain = gain_ref[pl.ds(group(u, cls), 1), :]
+                cl = cols(u, cls)
+                gu_ref[0, r, cl] = (
+                    gu_ref[0, r, cl].astype(F32) * gelu_slope(ub[slot, r, ln].astype(F32))
+                ).astype(BF)
                 slope = gelu_slope(vb[slot, r, ln].astype(F32))
                 scaled = gv_ref[0, r, cols(u, cls)].astype(F32)
                 e = sdn[u, r, ln].astype(F32) * gain

time: 107 us -> 101 us (0.944)
  Pallas kernels: 102 us -> 95.2 us
    pallas_call x1, Pallas kernels: 97.3 us -> 90.9 us  [on_device(): pl.pallas_call(kernel, out_shape=(jax.ShapeDtypeStruct(u_pre.shape, BF),...]
where the time goes in v3:
time: 101 us; the launch traced here: 100 us
  Pallas kernels  95.2 us (94%)
  local copies, waits for them, and re-layouts  4.35 us (4%)
    pallas_call x1, Pallas kernels, on_device(): pl.pallas_call(kernel, out_shape=(jax.ShapeDtypeStruct(u_pre.shape, BF),...  90.9 us
    unnamed x10, local copies, waits for them, and re-layouts  4.35 us
    pallas_call x1, Pallas kernels, on_device(): pl.pallas_call(place, out_shape=(jax.ShapeDtypeStruct(u_pre.shape, BF), j...  4.31 us

profile of v3, /device:TPU:0, one launch (start us, length us, event | category | flops | bytes accessed | tf_op | source)
XLA Modules:
  0.0 100.2 jit_solution(6063239020409096068)
XLA Ops:
  0.6 0.0 copy-start
  0.6 1.2 %copy-done = bf16[256,2048]{1,0:T(8,128)(2,1)S(1)} copy-done((bf16[256,2048]{1,0:T(8,128)(2,1)S(1)}, bf16[256,2048]{1,0:T(8,128)(2,1)}, u32[]{:S(2)}) %copy-start) | copy-done | bytes 1048600
  1.9 0.0 copy-start.1
  1.9 1.0 %copy-done.1 = bf16[16,128,128]{2,1,0:T(8,128)(2,1)S(1)} copy-done((bf16[16,128,128]{2,1,0:T(8,128)(2,1)S(1)}, bf16[16,128,128]{2,1,0:T(8,128)(2,1)}, u32[]{:S(2)}) %copy-start.1) | copy-done | bytes 524312
  2.9 0.0 copy-start.2
  2.9 0.7 copy-done.2
  3.6 0.0 copy-start.3
  3.6 0.7 copy-done.3
  4.3 0.0 copy-start.4
  4.3 0.7 copy-done.4
  5.0 90.9 %shard_map.135 = (bf16[1,1024,2048]{2,1,0:T(8,128)(2,1)S(1)}, bf16[1,1024,2048]{2,1,0:T(8,128)(2,1)S(1)}, f32[256,2048]{1,0:T(8,128)S(1)}, f32[16,128,128]{2,1,0:T(8,128)S(1)}, f32[3,16,128]{2,1,0:T(8,128)S(1)}) custom-call(bf16[1,1024,2048]{2,1,0:T(8,128)(2,1)} %u_hbm.1, bf16[1,1024,2048]{2,1,0:T(8,128)(2,1)} %v_hbm.1, bf16[1,1024,2048]{2,1,0:T(8,128)(2,1)} %d_hbm.1, ...), custom_call_target="tpu_custom_call" | custom-call | tf_op jit(solution)/shard_map/pallas_call | solution.py:655
  95.9 4.3 %shard_map.136 = (bf16[1,1024,2048]{2,1,0:T(8,128)(2,1)}, bf16[1,1024,2048]{2,1,0:T(8,128)(2,1)}, f32[256,2048]{1,0:T(8,128)}, f32[16,128,128]{2,1,0:T(8,128)}, ...) custom-call(bf16[1,1024,2048]{2,1,0:T(8,128)(2,1)S(1)} %get-tuple-element.12.gu, ...), custom_call_target="tpu_custom_call" | custom-call | tf_op jit(solution)/shard_map/pallas_call | solution.py:673
Async XLA Ops:
  0.6 1.2 %copy-start = (bf16[256,2048]{1,0:T(8,128)(2,1)S(1)}, bf16[256,2048]{1,0:T(8,128)(2,1)}, u32[]{:S(2)}) copy-start(bf16[256,2048]{1,0:T(8,128)(2,1)} %w_hbm.1) | copy-start | bytes 3145732
  1.9 1.0 %copy-start.1 = (bf16[16,128,128]{2,1,0:T(8,128)(2,1)S(1)}, bf16[16,128,128]{2,1,0:T(8,128)(2,1)}, u32[]{:S(2)}) copy-start(bf16[16,128,128]{2,1,0:T(8,128)(2,1)} %wm_hbm.1) | copy-start | bytes 1572868
  2.9 0.7 copy-start.2
  3.6 0.7 copy-start.3
  4.3 0.7 copy-start.4

commit v4 on v3

--- a/solution.py
+++ b/solution.py
@@ -59,13 +59,13 @@
 def kernel(
     u_hbm, v_hbm, d_hbm, wm_hbm, bias_hbm, gain_hbm, shift_hbm, w_hbm,
     gu_ref, gv_ref, gw_ref, gm_ref, stat_ref,
-    d_v, wbuf, ub, vb, gs, gt, pb, pr, tb, ra, rb, q, rc, rd, vx, rx, ob,
+    d_v, wbuf, ub, vb, gs, gt, pb, pr, tb, ct, ra, rb, rcy, q, rc, vx, rx, ob,
     qc, rc2, qd, rc3, cg, cp,
     st, st2, rs0, rs1, bias_ref, gain_ref, shift_ref, wl, wlt, bb, gwacc, bacc, gacc, sacc,
     sinv, sdn,
     ld_s, uv_s, wsend, wrecv, wrel_s, wrel_r,
     ps_s, ps_r, s1_s, s1_r, s2_s, s2_r, x_s, x_r, g1_s, g1_r, g2_s, g2_r,
-    c_s, c_r, t_s, t_r,
+    c_s, c_r, t_s, t_r, cy_s, cy_r,
 ):
     sp = lax.axis_index("sp")
     dp = lax.axis_index("dp")
@@ -178,8 +178,8 @@
     def ps(u):
         return rdma(pb.at[u % 2, o], pr.at[u % 2], ps_s.at[u % 2], ps_r.at[u], mate)
 
-    WAB = (1152, 1024)
-    OFF = (0, 1152)
+    WAB = (1024, 1024)
+    OFF = (0, 1024)
 
     def rows(j, half=None):
         if half is None:
@@ -207,24 +207,23 @@
             s1_s.at[u % 4, 1, ab, k], s1_r.at[u, 1, ab, k], first[ab](HOP[k]),
         )
 
-    def s2a(u, ab, k):
+    def s2(u, ab, d):
         return rdma(
-            q.at[u % 4, ab, pl.ds(16 * k, 16), lanes((i2[ab] + 2) % 4)],
-            rc.at[u, ab, k],
-            s2_s.at[u % 4, 0, ab, k], s2_r.at[u, 0, ab, k], second[ab](HOP[k]),
-        )
-
-    def s2b(u, ab, k):
+            q.at[u % 4, ab, :, lanes((i2[ab] + d) % 4)], rc.at[u, ab, d - 1],
+            s2_s.at[u % 4, ab, d - 1], s2_r.at[u, ab, d - 1], second[ab](d),
+        )
+
+    def cy(u, d):
         return rdma(
-            q.at[u % 4, ab, :, lanes((i2[ab] + HOP[k]) % 4)],
-            rd.at[u, ab, k],
-            s2_s.at[u % 4, 1, ab, k], s2_r.at[u, 1, ab, k], second[ab](HOP[k]),
+            ct.at[u % 4, rows((y + d) % 4)], rcy.at[u, d - 1],
+            cy_s.at[u % 4, d - 1], cy_r.at[u, d - 1], py(d),
         )
 
     def xs(u):
         xu, par, quad = unit(u, c)
         return rdma(vx.at[u], rx.at[par, quad], x_s.at[u], x_r.at[par, quad], dev(xu, y, z, c))
 
+    DS = (1, 2, 3)
     PAIRS = [(ab, d) for ab in range(2) for d in (1, 2, 3)]
     BOTH = [(ab, k) for ab in range(2) for k in range(2)]
 
@@ -234,13 +233,16 @@
 
         def body(i, _):
             r = pl.ds(al(i * 16, 16), 16)
-            for src, dst, w in ((0, 0, 1024), (WID, 1024, 128), (1024, 1152, 1024)):
-                tb[slot, r, pl.ds(dst, w)] = pb[u % 2, c, r, pl.ds(src, w)] + pr[u % 2, r, pl.ds(src, w)]
+            w, e = pl.ds(0, WID), pl.ds(WID, 128)
+            tb[slot, r, :] = pb[u % 2, c, r, w] + pr[u % 2, r, w]
+            ct[slot, r, :] = pb[u % 2, c, r, e] + pr[u % 2, r, e]
             return 0
 
         lax.fori_loop(0, 8, body, 0)
         for ab, k in BOTH:
             s1a(u, ab, k).start()
+        for d in DS:
+            cy(u, d).start()
 
     def do_s1b(u):
         slot = u % 4
@@ -251,10 +253,16 @@
             tb[slot, r, ln] = tb[slot, r, ln] + ra[u, ab, k, :, pl.ds(0, WAB[ab])]
         for ab, k in BOTH:
             s1b(u, ab, k).start()
+        for d in DS:
+            cy(u, d).wait()
+        xu, par, _ = unit(u, c)
+        acc = ct[slot, rows(y), :].astype(F32)
+        for k in range(3):
+            acc = acc + rcy[u, k].astype(F32)
+        qc[xu * 2 + par] = acc.astype(BF)
 
     def do_s2a(u):
         slot = u % 4
-        xu, par, _ = unit(u, c)
         for ab, k in BOTH:
             s1a(u, ab, k).wait_send()
             s1b(u, ab, k).wait()
@@ -269,30 +277,17 @@
                     return acc.astype(BF)
 
                 q[slot, ab, hs, :] = total(0, 1024)
-                if ab == 0:
-                    qc[xu * 2 + par, hs, :] = total(1024, 128)
-        for ab, k in BOTH:
-            s2a(u, ab, k).start()
-
-    def do_s2b(u):
-        slot = u % 4
-        for ab, k in BOTH:
-            s2a(u, ab, k).wait_recv()
-        for ab, k in BOTH:
-            hs, ln = pl.ds(16 * k, 16), lanes((i2[ab] + HOP[k]) % 4)
-            q[slot, ab, hs, ln] = q[slot, ab, hs, ln] + rc[u, ab, k]
-        for ab, k in BOTH:
-            s2b(u, ab, k).start()
+        for ab, d in PAIRS:
+            s2(u, ab, d).start()
 
     def do_x(u):
         slot = u % 4
-        for ab, k in BOTH:
-            s2a(u, ab, k).wait_send()
-            s2b(u, ab, k).wait()
+        for ab, d in PAIRS:
+            s2(u, ab, d).wait()
         for ab in range(2):
             acc = q[slot, ab, :, lanes(i2[ab])].astype(F32)
-            for k in range(2):
-                acc = acc + rd[u, ab, k].astype(F32)
+            for k in range(3):
+                acc = acc + rc[u, ab, k].astype(F32)
             vx[u, ab] = acc.astype(BF)
 
         @pl.when(u >= 2)
@@ -426,7 +421,7 @@
 
         lax.fori_loop(0, 8, block, 0, unroll=4)
 
-        for lag, act in ((5, do_x), (4, do_s2b), (3, do_s2a), (2, do_s1b), (1, do_ts)):
+        for lag, act in ((4, do_x), (3, do_s2a), (2, do_s1b), (1, do_ts)):
 
             @pl.when(u >= lag)
             def _(lag=lag, act=act):
@@ -510,10 +505,9 @@
         ref = cg.at[pl.ds(4 * k, 4), pl.ds(al(32 * j, 32), 32)]
         return rdma(ref, ref, c_s.at[0, k], c_r.at[0, k], py(HOP[k]))
 
-    DS = (1, 2, 3)
 
     def pipe(n):
-        for lag, act in ((5, do_x), (4, do_s2b), (3, do_s2a), (2, do_s1b), (1, do_ts)):
+        for lag, act in ((4, do_x), (3, do_s2a), (2, do_s1b), (1, do_ts)):
             if 0 <= n - lag <= 7:
                 act(n - lag)
 
@@ -533,14 +527,11 @@
         tstage(0, d, st2.at[0], py).start()
     finish(1)
     pipe(9)
+    for d in DS:
+        cz(d, (z + d) % 4).start()
     stat_step(0, py, pz)
     finish(2)
     pipe(10)
-    for d in DS:
-        cz(d, (z + d) % 4).start()
-    stat_step(1, pz, px)
-    finish(3)
-    pipe(11)
     for d in DS:
         cz(d, (z + d) % 4).wait()
     acc = qc[pl.ds(2 * z, 2)].astype(F32)
@@ -549,8 +540,9 @@
     qd[...] = acc.astype(BF)
     for d in DS:
         cx(d).start()
-    finish(4)
-    pipe(12)
+    stat_step(1, pz, px)
+    finish(3)
+    pipe(11)
     do_f(0)
     for d in DS:
         cx(d).wait()
@@ -565,26 +557,27 @@
     for k in range(3):
         tot = tot + rs1[2, k]
     stat_ref[...] = tot
-    finish(5)
+    finish(4)
     do_f(1)
     do_g2a(0)
     for d in DS:
         cgz(d, (z + 4 - d) % 4).wait_recv()
     for k in range(2):
         cga(k, y).start()
-    finish(6)
+    finish(5)
     do_g2a(1)
     do_g2b(0)
     for k in range(2):
         cga(k, (y + HOP[1 - k]) % 4).wait_recv()
     for k in range(2):
         cgb(k, (y + HOP[1 - k]) % 4).start()
-    finish(7)
+    finish(6)
     do_g2b(1)
     for k in range(2):
         cgb(k, (y + 2) % 4).wait_recv()
     swap = rdma(cg, cp, c_s.at[5, 0], c_r.at[5, 0], mate)
     swap.start()
+    finish(7)
     do_out(0)
 
     def gm_body(src, cls):
@@ -636,9 +629,9 @@
         V((1024, WID), BF), V((8, 2, 128, WID), BF),
         V((2, 1024, 256), BF), V((2, 1024, 256), BF),
         V((1024, 256), BF), V((256, 1024), BF),
-        V((2, 2, 128, EXT), BF), V((2, 128, EXT), BF), V((4, 128, EXT), BF),
-        V((8, 2, 2, 16, 1152), BF), V((8, 2, 2, 32, 1152), BF), V((4, 2, 32, 1024), BF),
-        V((8, 2, 2, 16, 256), BF), V((8, 2, 2, 32, 256), BF),
+        V((2, 2, 128, EXT), BF), V((2, 128, EXT), BF), V((4, 128, WID), BF), V((4, 128, 128), BF),
+        V((8, 2, 2, 16, 1024), BF), V((8, 2, 2, 32, 1024), BF), V((8, 3, 32, 128), BF), V((4, 2, 32, 1024), BF),
+        V((8, 2, 3, 32, 256), BF),
         V((8, 2, 32, 256), BF), V((2, 4, 2, 32, 256), BF), V((256, WID), BF),
         V((8, 32, 128), BF), V((3, 2, 32, 128), BF),
         V((2, 32, 128), BF), V((3, 2, 32, 128), BF), V((8, 128, 128), BF), V((8, 128, 128), BF),
@@ -648,9 +641,9 @@
         V((2, 128, 128), F32), V((2, 128, 128), F32), V((2, 8, 128), F32), V((2, 8, 128), F32),
         V((8, 1024, 256), BF), V((8, 1024, 256), BF),
         DMA((10,)), DMA((2, 2, 2)), DMA((6,)), DMA((6,)), DMA((8,)), DMA((8,)),
-        DMA((2,)), DMA((8,)), DMA((4, 2, 2, 2)), DMA((8, 2, 2, 2)), DMA((4, 2, 2, 2)), DMA((8, 2, 2, 2)),
+        DMA((2,)), DMA((8,)), DMA((4, 2, 2, 2)), DMA((8, 2, 2, 2)), DMA((4, 2, 3)), DMA((8, 2, 3)),
         DMA((8,)), DMA((2, 4)), DMA((2, 2, 3)), DMA((2, 2, 3)), DMA((2, 2, 2, 2)), DMA((2, 2, 2, 2)),
-        DMA((6, 3)), DMA((6, 3)), DMA((4, 3)), DMA((4, 3)),
+        DMA((6, 3)), DMA((6, 3)), DMA((4, 3)), DMA((4, 3)), DMA((4, 3)), DMA((8, 3)),
     ]
     outs = pl.pallas_call(
         kernel,

time: 101 us -> 97.8 us (0.968)
  Pallas kernels: 95.2 us -> 92.5 us
    pallas_call x1, Pallas kernels: 90.9 us -> 88.2 us  [on_device(): pl.pallas_call(kernel, out_shape=(jax.ShapeDtypeStruct(u_pre.shape, BF),...]
where the time goes in v4:
time: 97.8 us; the launch traced here: 97.5 us
  Pallas kernels  92.5 us (95%)
  local copies, waits for them, and re-layouts  4.35 us (4%)
    pallas_call x1, Pallas kernels, on_device(): pl.pallas_call(kernel, out_shape=(jax.ShapeDtypeStruct(u_pre.shape, BF),...  88.2 us
    unnamed x10, local copies, waits for them, and re-layouts  4.35 us
    pallas_call x1, Pallas kernels, on_device(): pl.pallas_call(place, out_shape=(jax.ShapeDtypeStruct(u_pre.shape, BF), j...  4.31 us

profile of v4, /device:TPU:0, one launch (start us, length us, event | category | flops | bytes accessed | tf_op | source)
XLA Modules:
  0.0 97.5 jit_solution(10996147363136323993)
XLA Ops:
  0.6 0.0 copy-start
  0.6 1.2 %copy-done = bf16[256,2048]{1,0:T(8,128)(2,1)S(1)} copy-done((bf16[256,2048]{1,0:T(8,128)(2,1)S(1)}, bf16[256,2048]{1,0:T(8,128)(2,1)}, u32[]{:S(2)}) %copy-start) | copy-done | bytes 1048600
  1.9 0.0 copy-start.1
  1.9 1.0 %copy-done.1 = bf16[16,128,128]{2,1,0:T(8,128)(2,1)S(1)} copy-done((bf16[16,128,128]{2,1,0:T(8,128)(2,1)S(1)}, bf16[16,128,128]{2,1,0:T(8,128)(2,1)}, u32[]{:S(2)}) %copy-start.1) | copy-done | bytes 524312
  2.9 0.0 copy-start.2
  2.9 0.7 copy-done.2
  3.6 0.0 copy-start.3
  3.6 0.7 copy-done.3
  4.3 0.0 copy-start.4
  4.3 0.7 copy-done.4
  5.0 88.2 %shard_map.135 = (bf16[1,1024,2048]{2,1,0:T(8,128)(2,1)S(1)}, bf16[1,1024,2048]{2,1,0:T(8,128)(2,1)S(1)}, f32[256,2048]{1,0:T(8,128)S(1)}, f32[16,128,128]{2,1,0:T(8,128)S(1)}, f32[3,16,128]{2,1,0:T(8,128)S(1)}) custom-call(bf16[1,1024,2048]{2,1,0:T(8,128)(2,1)} %u_hbm.1, bf16[1,1024,2048]{2,1,0:T(8,128)(2,1)} %v_hbm.1, bf16[1,1024,2048]{2,1,0:T(8,128)(2,1)} %d_hbm.1, ...), custom_call_target="tpu_custom_call" | custom-call | tf_op jit(solution)/shard_map/pallas_call | solution.py:648
  93.2 4.3 %shard_map.136 = (bf16[1,1024,2048]{2,1,0:T(8,128)(2,1)}, bf16[1,1024,2048]{2,1,0:T(8,128)(2,1)}, f32[256,2048]{1,0:T(8,128)}, f32[16,128,128]{2,1,0:T(8,128)}, ...) custom-call(bf16[1,1024,2048]{2,1,0:T(8,128)(2,1)S(1)} %get-tuple-element.12.gu, ...), custom_call_target="tpu_custom_call" | custom-call | tf_op jit(solution)/shard_map/pallas_call | solution.py:666
Async XLA Ops:
  0.6 1.2 %copy-start = (bf16[256,2048]{1,0:T(8,128)(2,1)S(1)}, bf16[256,2048]{1,0:T(8,128)(2,1)}, u32[]{:S(2)}) copy-start(bf16[256,2048]{1,0:T(8,128)(2,1)} %w_hbm.1) | copy-start | bytes 3145732
  1.9 1.0 %copy-start.1 = (bf16[16,128,128]{2,1,0:T(8,128)(2,1)S(1)}, bf16[16,128,128]{2,1,0:T(8,128)(2,1)}, u32[]{:S(2)}) copy-start(bf16[16,128,128]{2,1,0:T(8,128)(2,1)} %wm_hbm.1) | copy-start | bytes 1572868
  2.9 0.7 copy-start.2
  3.6 0.7 copy-start.3
  4.3 0.7 copy-start.4

commit v5 on v4

--- a/solution.py
+++ b/solution.py
@@ -372,10 +372,6 @@
                 cpy.start()
 
         gs[...] = dot_nt(d_v[...], wbuf[u].reshape(256, WID)).astype(BF)
-
-        @pl.when((u >= 1) & (u < 7))
-        def _():
-            arrive(u + 1)
 
 
         for cpy in uv_copies(u):
@@ -420,6 +416,10 @@
             return 0
 
         lax.fori_loop(0, 8, block, 0, unroll=4)
+
+        @pl.when((u >= 1) & (u < 7))
+        def _():
+            arrive(u + 1)
 
         for lag, act in ((4, do_x), (3, do_s2a), (2, do_s1b), (1, do_ts)):
 

time: 97.8 us -> 97.3 us (level)
  no operation moved by 1% of the time
where the time goes in v5:
time: 97.3 us; the launch traced here: 96.9 us
  Pallas kernels  91.9 us (94%)
  local copies, waits for them, and re-layouts  4.35 us (4%)
    pallas_call x1, Pallas kernels, on_device(): pl.pallas_call(kernel, out_shape=(jax.ShapeDtypeStruct(u_pre.shape, BF),...  87.6 us
    unnamed x10, local copies, waits for them, and re-layouts  4.35 us
    pallas_call x1, Pallas kernels, on_device(): pl.pallas_call(place, out_shape=(jax.ShapeDtypeStruct(u_pre.shape, BF), j...  4.31 us

profile of v5, /device:TPU:0, one launch (start us, length us, event | category | flops | bytes accessed | tf_op | source)
XLA Modules:
  0.0 96.9 jit_solution(9416255694664081559)
XLA Ops:
  0.6 0.0 copy-start
  0.6 1.2 %copy-done = bf16[256,2048]{1,0:T(8,128)(2,1)S(1)} copy-done((bf16[256,2048]{1,0:T(8,128)(2,1)S(1)}, bf16[256,2048]{1,0:T(8,128)(2,1)}, u32[]{:S(2)}) %copy-start) | copy-done | bytes 1048600
  1.9 0.0 copy-start.1
  1.9 1.0 %copy-done.1 = bf16[16,128,128]{2,1,0:T(8,128)(2,1)S(1)} copy-done((bf16[16,128,128]{2,1,0:T(8,128)(2,1)S(1)}, bf16[16,128,128]{2,1,0:T(8,128)(2,1)}, u32[]{:S(2)}) %copy-start.1) | copy-done | bytes 524312
  2.9 0.0 copy-start.2
  2.9 0.7 copy-done.2
  3.6 0.0 copy-start.3
  3.6 0.7 copy-done.3
  4.3 0.0 copy-start.4
  4.3 0.7 copy-done.4
  5.0 87.6 %shard_map.135 = (bf16[1,1024,2048]{2,1,0:T(8,128)(2,1)S(1)}, bf16[1,1024,2048]{2,1,0:T(8,128)(2,1)S(1)}, f32[256,2048]{1,0:T(8,128)S(1)}, f32[16,128,128]{2,1,0:T(8,128)S(1)}, f32[3,16,128]{2,1,0:T(8,128)S(1)}) custom-call(bf16[1,1024,2048]{2,1,0:T(8,128)(2,1)} %u_hbm.1, bf16[1,1024,2048]{2,1,0:T(8,128)(2,1)} %v_hbm.1, bf16[1,1024,2048]{2,1,0:T(8,128)(2,1)} %d_hbm.1, ...), custom_call_target="tpu_custom_call" | custom-call | tf_op jit(solution)/shard_map/pallas_call | solution.py:648
  92.6 4.3 %shard_map.136 = (bf16[1,1024,2048]{2,1,0:T(8,128)(2,1)}, bf16[1,1024,2048]{2,1,0:T(8,128)(2,1)}, f32[256,2048]{1,0:T(8,128)}, f32[16,128,128]{2,1,0:T(8,128)}, ...) custom-call(bf16[1,1024,2048]{2,1,0:T(8,128)(2,1)S(1)} %get-tuple-element.12.gu, ...), custom_call_target="tpu_custom_call" | custom-call | tf_op jit(solution)/shard_map/pallas_call | solution.py:666
Async XLA Ops:
  0.6 1.2 %copy-start = (bf16[256,2048]{1,0:T(8,128)(2,1)S(1)}, bf16[256,2048]{1,0:T(8,128)(2,1)}, u32[]{:S(2)}) copy-start(bf16[256,2048]{1,0:T(8,128)(2,1)} %w_hbm.1) | copy-start | bytes 3145732
  1.9 1.0 %copy-start.1 = (bf16[16,128,128]{2,1,0:T(8,128)(2,1)S(1)}, bf16[16,128,128]{2,1,0:T(8,128)(2,1)}, u32[]{:S(2)}) copy-start(bf16[16,128,128]{2,1,0:T(8,128)(2,1)} %wm_hbm.1) | copy-start | bytes 1572868
  2.9 0.7 copy-start.2
  3.6 0.7 copy-start.3
  4.3 0.7 copy-start.4
